TPU v7x, 512 devices: a whole 4x8x8 slice. The times are simulated.
512 devices in a mesh: sp: 64 (over z, y), fs: 4 (over x), tp: 2 (over core).
Axes of the slice: x: 4, y: 8, z: 8, core: 2. Of those that a mesh axis runs over, the one named last changes fastest.
Arguments:
- tokens: bfloat16 [16384, 2048], P(('sp', 'fs', 'tp')), may hold values from -6 to 6
- norm_gain: float32 [2048], replicated, may hold values from 0.1 to 1.9
- w_query: bfloat16 [2048, 1024], P(None, ('fs', 'tp')), may hold values from -0.125 to 0.125
- w_key: bfloat16 [2048, 1024], P(None, ('fs', 'tp')), may hold values from -0.125 to 0.125
- w_value: bfloat16 [2048, 1024], P(None, ('fs', 'tp')), may hold values from -0.125 to 0.125
- w_pool: bfloat16 [2048, 1024], P(None, ('fs', 'tp')), may hold values from -0.125 to 0.125
- query_gain: float32 [64], replicated, may hold values from 1.2 to 1.6
- key_gain: float32 [64], replicated, may hold values from 1.2 to 1.6
- lambdas: float32 [8], P(('fs', 'tp')), may hold values from 0.3 to 0.8
- head_gain: float32 [128], replicated, may hold values from 0.1 to 1.9
- w_out_attn: bfloat16 [1024, 2048], P(('fs', 'tp')), may hold values from -0.125 to 0.125
- w_out_pool: bfloat16 [1024, 2048], P(('fs', 'tp')), may hold values from -0.125 to 0.125
Outputs:
- layer_out: bfloat16 [16384, 2048], P(('sp', 'fs', 'tp'))
All inputs are finite; a program needn't handle non-finite values.
Results may differ from a plain program's by a relative error of at most 0.015.
Values may be sent and summed in bfloat16 or wider, within the bound.
No kernel may reach another device: no remote copies, remote signals or barrier semaphores. Data moves between devices by JAX's collectives and lax.ppermute only.
A program may use at most 128 MiB of HBM per device.

v0:
```python
import math

import jax
import jax.numpy as jnp
from jax import lax
from jax.sharding import PartitionSpec as P

HEAD_DIM = 64
POOL_GROUP_DIM = 256
POOL_SPAN = 16


epsilon = 1e-06
windows = (2, 4, 8, 16)


def copy_for_each(x, axis):
    copies = jnp.broadcast_to(x, (lax.axis_size(axis), *x.shape))
    return lax.all_to_all(copies, axis, split_axis=0, concat_axis=0, tiled=True)


def laid_out(tiles, dim):
    tiles = jnp.moveaxis(tiles, 0, dim)
    dims = tiles.shape
    return tiles.reshape(*dims[:dim], dims[dim] * dims[dim + 1], *dims[dim + 2 :])


def gathered_copies(x, axis, dim):
    tiles = copy_for_each(x, axis)
    return laid_out(tiles, dim)


def side_by_side(arrays, axis, dim, along):
    both = jnp.concatenate(arrays, axis=along)
    filled, at, done = (lax.all_gather(both, axis, axis=dim, tiled=True), 0, [])
    for a in arrays:
        done.append(lax.slice_in_dim(filled, at, at + a.shape[along], axis=along))
        at += a.shape[along]
    return tuple(done)


def from_behind(x, axis, by):
    devices = lax.axis_size(axis)
    pairs = [(i, i + by) for i in range(devices) if 0 <= i + by < devices]
    return lax.ppermute(x, axis, pairs)


def rms_scale(values, gain):
    return values * lax.rsqrt(jnp.mean(values * values, axis=-1, keepdims=True) + epsilon) * gain


def body(
    tokens,
    norm_gain,
    w_query,
    w_key,
    w_value,
    w_pool,
    query_gain,
    key_gain,
    lambdas,
    head_gain,
    w_out_attn,
    w_out_pool,
):
    normed = rms_scale(tokens.astype(jnp.float32), norm_gain).astype(jnp.bfloat16)
    in_weights = jnp.concatenate([w_query, w_key, w_value, w_pool], axis=1)
    projected = jnp.dot(
        gathered_copies(normed, ("fs", "tp"), 0), in_weights, preferred_element_type=jnp.float32
    )
    own_rows = projected.shape[0]
    heads_dev = lambdas.shape[0]
    value_dim = head_gain.shape[0]
    query_cols = w_query.shape[1]
    value_cols = w_value.shape[1]
    query_raw = projected[:, :query_cols].reshape(own_rows, heads_dev, 2, HEAD_DIM)
    key_raw = projected[:, query_cols : 2 * query_cols].reshape(own_rows, heads_dev, 2, HEAD_DIM)
    queries = rms_scale(query_raw, query_gain).astype(jnp.bfloat16)
    keys_flat = rms_scale(key_raw, key_gain).astype(jnp.bfloat16).reshape(own_rows, query_cols)
    values = projected[:, 2 * query_cols : 2 * query_cols + value_cols].astype(jnp.bfloat16)
    pool_input = projected[:, 2 * query_cols + value_cols :].astype(jnp.bfloat16)
    query_first = lax.axis_index("sp") * own_rows
    query_pos = query_first + jnp.arange(own_rows, dtype=jnp.int32)
    groups = [(queries, query_pos)]
    score_scale = HEAD_DIM ** (-0.5)
    start_state = tuple(
        (
            (
                jnp.zeros((heads_dev, 2, grp[0].shape[0], value_dim), jnp.float32),
                jnp.zeros((heads_dev, 2, grp[0].shape[0]), jnp.float32),
            )
            for grp in groups
        )
    )
    key_rows, value_rows = side_by_side((keys_flat, values), "sp", 0, 1)
    key_count = key_rows.shape[0]
    block_rows = math.gcd(key_count, 4 * own_rows)
    key_heads = key_rows.reshape(key_count, heads_dev, 2, HEAD_DIM)
    value_heads = value_rows.reshape(key_count, heads_dev, value_dim)

    def one_block(index, state):
        key_first = index * block_rows
        key_block = lax.dynamic_slice_in_dim(key_heads, index * block_rows, block_rows, 0)
        value_block = lax.dynamic_slice_in_dim(value_heads, index * block_rows, block_rows, 0)
        key_pos = key_first + jnp.arange(block_rows, dtype=jnp.int32)
        updated = []
        for group_rows, group_state in zip(groups, state):
            group_queries, group_pos = group_rows

            def compute(inner, group_queries=group_queries, group_pos=group_pos):
                scores = (
                    jnp.einsum(
                        "qhcd,khcd->hcqk",
                        group_queries,
                        key_block,
                        preferred_element_type=jnp.float32,
                    )
                    * score_scale
                )
                visible = key_pos[None, :] <= group_pos[:, None]
                expo = jnp.where(visible[None, None], jnp.exp(scores), 0.0)
                totals = inner[1] + jnp.sum(expo, axis=3)
                numerators = inner[0] + jnp.einsum(
                    "hcqk,khe->hcqe",
                    expo.astype(jnp.bfloat16),
                    value_block,
                    preferred_element_type=jnp.float32,
                )
                return (numerators, totals)

            def unchanged(inner):
                return inner

            updated.append(
                lax.cond(key_first <= jnp.max(group_pos), compute, unchanged, group_state)
            )
        return tuple(updated)

    states = lax.fori_loop(0, key_count // block_rows, one_block, start_state)
    numerators, totals = states[0]
    row_count = numerators.shape[2]
    head_out = (
        numerators[:, 0] / totals[:, 0, :, None]
        - lambdas[:, None, None] * numerators[:, 1] / totals[:, 1, :, None]
    )
    normed_heads = rms_scale(head_out, head_gain).astype(jnp.bfloat16)
    attended = jnp.transpose(normed_heads, (1, 0, 2)).reshape(row_count, heads_dev * value_dim)
    pool_cols = pool_input.shape[1]
    pool_group = lax.axis_index(("fs", "tp")) * pool_cols // POOL_GROUP_DIM
    window_size = jnp.sum(
        jnp.where(
            jnp.arange(len(windows), dtype=jnp.int32) == pool_group,
            jnp.array(windows, jnp.int32),
            0,
        )
    )
    reach = POOL_SPAN - 1
    earlier = from_behind(pool_input[own_rows - reach :], "sp", 1)
    extended = jnp.concatenate([earlier, pool_input], axis=0).astype(jnp.float32)
    window_sum = jnp.zeros((own_rows, pool_cols), jnp.float32)
    for offset in range(POOL_SPAN):
        window_sum = window_sum + jnp.where(
            offset < window_size, extended[reach - offset : reach - offset + own_rows], 0.0
        )
    divisor = jnp.minimum((query_pos + 1).astype(jnp.float32), window_size.astype(jnp.float32))[
        :, None
    ]
    pooled = (window_sum / divisor - extended[reach:]).astype(jnp.bfloat16)
    devices = lax.axis_size(("fs", "tp"))
    out_rows = own_rows // devices
    attn_cols = attended.shape[1]
    mixed_local = jnp.concatenate([attended, pooled], axis=1)
    regrouped = lax.all_to_all(mixed_local, ("fs", "tp"), split_axis=0, concat_axis=1, tiled=True)
    blocks = regrouped.reshape(out_rows, devices, attn_cols + pool_cols)
    attn_piece, pool_piece = side_by_side((w_out_attn, w_out_pool), ("fs", "tp"), 0, 1)
    span_count = attn_piece.shape[0] // attn_cols
    attn_left = blocks[:, :, :attn_cols].reshape(out_rows, span_count * attn_cols)
    pool_left = blocks[:, :, attn_cols:].reshape(out_rows, span_count * pool_cols)
    summed = jnp.dot(attn_left, attn_piece, preferred_element_type=jnp.float32)
    summed = summed + jnp.dot(pool_left, pool_piece, preferred_element_type=jnp.float32)
    return summed.astype(jnp.bfloat16)


def solution(mesh):
    return jax.shard_map(
        body,
        mesh=mesh,
        in_specs=(
            P(("sp", "fs", "tp"), None),
            P(),
            P(None, ("fs", "tp")),
            P(None, ("fs", "tp")),
            P(None, ("fs", "tp")),
            P(None, ("fs", "tp")),
            P(),
            P(),
            P(("fs", "tp")),
            P(),
            P(("fs", "tp"), None),
            P(("fs", "tp"), None),
        ),
        out_specs=P(("sp", "fs", "tp"), None),
        check_vma=False,
    )
```

profile of v0, /device:TPU:488, one launch (start us, length us, event | category | flops | bytes accessed | tf_op | source)
XLA Modules:
  0.0 231.8 jit_solution(7383733650758047698)
XLA Ops:
  9.7 4.3 %all-to-all-start = ((bf16[8,32,2048]{2,1,0:T(8,128)(2,1)}), bf16[8,32,2048]{2,1,0:T(8,128)(2,1)S(1)}, u32[]{:S(2)}, u32[]{:S(2)}) async-start(bf16[8,32,2048]{2,1,0:T(8,128)(2,1)} %broadcast_in_dim.59), calls=%async_computation | async-start | bytes 2097152 | tf_op jit(solution)/shard_map/all_to_all | solution.py:19
  14.8 15.1 %all-to-all-done = bf16[8,32,2048]{2,1,0:T(8,128)(2,1)S(1)} async-done(((bf16[8,32,2048]{2,1,0:T(8,128)(2,1)}), bf16[8,32,2048]{2,1,0:T(8,128)(2,1)S(1)}, u32[]{:S(2)}, u32[]{:S(2)}) %all-to-all-start) | async-done | bytes 1048608 | tf_op jit(solution)/shard_map/all_to_all | solution.py:19
  52.1 75.1 %all-gather.3.cloned.1.call-done = bf16[16384,256]{1,0:T(8,128)(2,1)} async-done(((bf16[256,256]{1,0:T(8,128)(2,1)}), bf16[16384,256]{1,0:T(8,128)(2,1)}) %all-gather.3.cloned.1.call-update) | async-done | bytes 8388624 | tf_op jit(solution)/shard_map/all_gather | solution.py:35
  127.2 5.7 %slice_bitcast_fusion = (bf16[16384,1,128]{2,0,1:T(8,128)(2,1)}, bf16[16384,128]{1,0:T(8,128)(2,1)}) fusion(bf16[16384,256]{1,0:T(8,128)(2,1)} %all-gather.3.cloned.1.call-done), kind=kLoop, calls=%fused_computation.27 | loop fusion | bytes 16777216 | tf_op jit(solution)/shard_map/reshape | solution.py:99
  132.9 6.4 %copy.42 = bf16[16384,128]{0,1:T(8,128)(2,1)} copy(bf16[16384,128]{1,0:T(8,128)(2,1)} %get-tuple-element.332) | data formatting | bytes 8388608 | tf_op jit(solution)/shard_map/slice | solution.py:37
  139.4 67.9 %while.17 = (s32[]{:T(128)}, f32[1,2,256,128]{3,2,1,0:T(8,128)S(1)}, f32[1,2,256]{2,1,0:T(2,128)S(1)}, s32[]{:T(128)}, bf16[16384,1,2,64]{0,3,2,1:T(8,128)(2,1)}...) while((s32[]{:T(128)}, ...), condition=%wide.region_8.9_spmd.clone, body=%wide.region_4.8_spmd.clone.sunk | while | flops 204801280 | bytes 6123809 | solution.py:139
  140.2 3.5 %conditional.3 = ((f32[1,2,256,128]{3,2,1,0:T(8,128)S(1)}, f32[1,2,256]{2,1,0:T(2,128)S(1)})) conditional(s32[]{:T(128)} %convert_element_type.96, (f32[1,2,256,128]{3,2,1,0:T(8,128)S(1)}, f32[1,2,256]{2,1,0:T(2,128)S(1)}) %tuple.66, (s32[]{:T(128)}, s32[1024]{0:T(1024)S(1)}, s32[]{:T(128)}, bf16[16384,1,2,64]{0,3,2,1:T(8,128)(2,1)}, ...), branch_computations={%region_5.0_spmd, %region_6.7_spmd} | conditional | flops 204801280 | bytes 6118474 | solution.py:135
  144.4 3.5 %conditional.3 = ((f32[1,2,256,128]{3,2,1,0:T(8,128)S(1)}, f32[1,2,256]{2,1,0:T(2,128)S(1)})) conditional(s32[]{:T(128)} %convert_element_type.96, (f32[1,2,256,128]{3,2,1,0:T(8,128)S(1)}, f32[1,2,256]{2,1,0:T(2,128)S(1)}) %tuple.66, (s32[]{:T(128)}, s32[1024]{0:T(1024)S(1)}, s32[]{:T(128)}, bf16[16384,1,2,64]{0,3,2,1:T(8,128)(2,1)}, ...), branch_computations={%region_5.0_spmd, %region_6.7_spmd} | conditional | flops 204801280 | bytes 6118474 | solution.py:135
  148.6 3.5 %conditional.3 = ((f32[1,2,256,128]{3,2,1,0:T(8,128)S(1)}, f32[1,2,256]{2,1,0:T(2,128)S(1)})) conditional(s32[]{:T(128)} %convert_element_type.96, (f32[1,2,256,128]{3,2,1,0:T(8,128)S(1)}, f32[1,2,256]{2,1,0:T(2,128)S(1)}) %tuple.66, (s32[]{:T(128)}, s32[1024]{0:T(1024)S(1)}, s32[]{:T(128)}, bf16[16384,1,2,64]{0,3,2,1:T(8,128)(2,1)}, ...), branch_computations={%region_5.0_spmd, %region_6.7_spmd} | conditional | flops 204801280 | bytes 6118474 | solution.py:135
  152.9 3.5 %conditional.3 = ((f32[1,2,256,128]{3,2,1,0:T(8,128)S(1)}, f32[1,2,256]{2,1,0:T(2,128)S(1)})) conditional(s32[]{:T(128)} %convert_element_type.96, (f32[1,2,256,128]{3,2,1,0:T(8,128)S(1)}, f32[1,2,256]{2,1,0:T(2,128)S(1)}) %tuple.66, (s32[]{:T(128)}, s32[1024]{0:T(1024)S(1)}, s32[]{:T(128)}, bf16[16384,1,2,64]{0,3,2,1:T(8,128)(2,1)}, ...), branch_computations={%region_5.0_spmd, %region_6.7_spmd} | conditional | flops 204801280 | bytes 6118474 | solution.py:135
  157.2 3.5 %conditional.3 = ((f32[1,2,256,128]{3,2,1,0:T(8,128)S(1)}, f32[1,2,256]{2,1,0:T(2,128)S(1)})) conditional(s32[]{:T(128)} %convert_element_type.96, (f32[1,2,256,128]{3,2,1,0:T(8,128)S(1)}, f32[1,2,256]{2,1,0:T(2,128)S(1)}) %tuple.66, (s32[]{:T(128)}, s32[1024]{0:T(1024)S(1)}, s32[]{:T(128)}, bf16[16384,1,2,64]{0,3,2,1:T(8,128)(2,1)}, ...), branch_computations={%region_5.0_spmd, %region_6.7_spmd} | conditional | flops 204801280 | bytes 6118474 | solution.py:135
  161.4 3.5 %conditional.3 = ((f32[1,2,256,128]{3,2,1,0:T(8,128)S(1)}, f32[1,2,256]{2,1,0:T(2,128)S(1)})) conditional(s32[]{:T(128)} %convert_element_type.96, (f32[1,2,256,128]{3,2,1,0:T(8,128)S(1)}, f32[1,2,256]{2,1,0:T(2,128)S(1)}) %tuple.66, (s32[]{:T(128)}, s32[1024]{0:T(1024)S(1)}, s32[]{:T(128)}, bf16[16384,1,2,64]{0,3,2,1:T(8,128)(2,1)}, ...), branch_computations={%region_5.0_spmd, %region_6.7_spmd} | conditional | flops 204801280 | bytes 6118474 | solution.py:135
  165.7 3.5 %conditional.3 = ((f32[1,2,256,128]{3,2,1,0:T(8,128)S(1)}, f32[1,2,256]{2,1,0:T(2,128)S(1)})) conditional(s32[]{:T(128)} %convert_element_type.96, (f32[1,2,256,128]{3,2,1,0:T(8,128)S(1)}, f32[1,2,256]{2,1,0:T(2,128)S(1)}) %tuple.66, (s32[]{:T(128)}, s32[1024]{0:T(1024)S(1)}, s32[]{:T(128)}, bf16[16384,1,2,64]{0,3,2,1:T(8,128)(2,1)}, ...), branch_computations={%region_5.0_spmd, %region_6.7_spmd} | conditional | flops 204801280 | bytes 6118474 | solution.py:135
  169.9 3.5 %conditional.3 = ((f32[1,2,256,128]{3,2,1,0:T(8,128)S(1)}, f32[1,2,256]{2,1,0:T(2,128)S(1)})) conditional(s32[]{:T(128)} %convert_element_type.96, (f32[1,2,256,128]{3,2,1,0:T(8,128)S(1)}, f32[1,2,256]{2,1,0:T(2,128)S(1)}) %tuple.66, (s32[]{:T(128)}, s32[1024]{0:T(1024)S(1)}, s32[]{:T(128)}, bf16[16384,1,2,64]{0,3,2,1:T(8,128)(2,1)}, ...), branch_computations={%region_5.0_spmd, %region_6.7_spmd} | conditional | flops 204801280 | bytes 6118474 | solution.py:135
  174.1 3.5 %conditional.3 = ((f32[1,2,256,128]{3,2,1,0:T(8,128)S(1)}, f32[1,2,256]{2,1,0:T(2,128)S(1)})) conditional(s32[]{:T(128)} %convert_element_type.96, (f32[1,2,256,128]{3,2,1,0:T(8,128)S(1)}, f32[1,2,256]{2,1,0:T(2,128)S(1)}) %tuple.66, (s32[]{:T(128)}, s32[1024]{0:T(1024)S(1)}, s32[]{:T(128)}, bf16[16384,1,2,64]{0,3,2,1:T(8,128)(2,1)}, ...), branch_computations={%region_5.0_spmd, %region_6.7_spmd} | conditional | flops 204801280 | bytes 6118474 | solution.py:135
  178.4 3.5 %conditional.3 = ((f32[1,2,256,128]{3,2,1,0:T(8,128)S(1)}, f32[1,2,256]{2,1,0:T(2,128)S(1)})) conditional(s32[]{:T(128)} %convert_element_type.96, (f32[1,2,256,128]{3,2,1,0:T(8,128)S(1)}, f32[1,2,256]{2,1,0:T(2,128)S(1)}) %tuple.66, (s32[]{:T(128)}, s32[1024]{0:T(1024)S(1)}, s32[]{:T(128)}, bf16[16384,1,2,64]{0,3,2,1:T(8,128)(2,1)}, ...), branch_computations={%region_5.0_spmd, %region_6.7_spmd} | conditional | flops 204801280 | bytes 6118474 | solution.py:135
  182.6 3.5 %conditional.3 = ((f32[1,2,256,128]{3,2,1,0:T(8,128)S(1)}, f32[1,2,256]{2,1,0:T(2,128)S(1)})) conditional(s32[]{:T(128)} %convert_element_type.96, (f32[1,2,256,128]{3,2,1,0:T(8,128)S(1)}, f32[1,2,256]{2,1,0:T(2,128)S(1)}) %tuple.66, (s32[]{:T(128)}, s32[1024]{0:T(1024)S(1)}, s32[]{:T(128)}, bf16[16384,1,2,64]{0,3,2,1:T(8,128)(2,1)}, ...), branch_computations={%region_5.0_spmd, %region_6.7_spmd} | conditional | flops 204801280 | bytes 6118474 | solution.py:135
  186.9 3.5 %conditional.3 = ((f32[1,2,256,128]{3,2,1,0:T(8,128)S(1)}, f32[1,2,256]{2,1,0:T(2,128)S(1)})) conditional(s32[]{:T(128)} %convert_element_type.96, (f32[1,2,256,128]{3,2,1,0:T(8,128)S(1)}, f32[1,2,256]{2,1,0:T(2,128)S(1)}) %tuple.66, (s32[]{:T(128)}, s32[1024]{0:T(1024)S(1)}, s32[]{:T(128)}, bf16[16384,1,2,64]{0,3,2,1:T(8,128)(2,1)}, ...), branch_computations={%region_5.0_spmd, %region_6.7_spmd} | conditional | flops 204801280 | bytes 6118474 | solution.py:135
  191.1 3.5 %conditional.3 = ((f32[1,2,256,128]{3,2,1,0:T(8,128)S(1)}, f32[1,2,256]{2,1,0:T(2,128)S(1)})) conditional(s32[]{:T(128)} %convert_element_type.96, (f32[1,2,256,128]{3,2,1,0:T(8,128)S(1)}, f32[1,2,256]{2,1,0:T(2,128)S(1)}) %tuple.66, (s32[]{:T(128)}, s32[1024]{0:T(1024)S(1)}, s32[]{:T(128)}, bf16[16384,1,2,64]{0,3,2,1:T(8,128)(2,1)}, ...), branch_computations={%region_5.0_spmd, %region_6.7_spmd} | conditional | flops 204801280 | bytes 6118474 | solution.py:135
  195.3 3.5 %conditional.3 = ((f32[1,2,256,128]{3,2,1,0:T(8,128)S(1)}, f32[1,2,256]{2,1,0:T(2,128)S(1)})) conditional(s32[]{:T(128)} %convert_element_type.96, (f32[1,2,256,128]{3,2,1,0:T(8,128)S(1)}, f32[1,2,256]{2,1,0:T(2,128)S(1)}) %tuple.66, (s32[]{:T(128)}, s32[1024]{0:T(1024)S(1)}, s32[]{:T(128)}, bf16[16384,1,2,64]{0,3,2,1:T(8,128)(2,1)}, ...), branch_computations={%region_5.0_spmd, %region_6.7_spmd} | conditional | flops 204801280 | bytes 6118474 | solution.py:135
  199.6 3.5 %conditional.3 = ((f32[1,2,256,128]{3,2,1,0:T(8,128)S(1)}, f32[1,2,256]{2,1,0:T(2,128)S(1)})) conditional(s32[]{:T(128)} %convert_element_type.96, (f32[1,2,256,128]{3,2,1,0:T(8,128)S(1)}, f32[1,2,256]{2,1,0:T(2,128)S(1)}) %tuple.66, (s32[]{:T(128)}, s32[1024]{0:T(1024)S(1)}, s32[]{:T(128)}, bf16[16384,1,2,64]{0,3,2,1:T(8,128)(2,1)}, ...), branch_computations={%region_5.0_spmd, %region_6.7_spmd} | conditional | flops 204801280 | bytes 6118474 | solution.py:135
  203.8 3.5 %conditional.3 = ((f32[1,2,256,128]{3,2,1,0:T(8,128)S(1)}, f32[1,2,256]{2,1,0:T(2,128)S(1)})) conditional(s32[]{:T(128)} %convert_element_type.96, (f32[1,2,256,128]{3,2,1,0:T(8,128)S(1)}, f32[1,2,256]{2,1,0:T(2,128)S(1)}) %tuple.66, (s32[]{:T(128)}, s32[1024]{0:T(1024)S(1)}, s32[]{:T(128)}, bf16[16384,1,2,64]{0,3,2,1:T(8,128)(2,1)}, ...), branch_computations={%region_5.0_spmd, %region_6.7_spmd} | conditional | flops 204801280 | bytes 6118474 | solution.py:135
  208.0 10.1 %all_to_all.18 = bf16[8,32,256]{2,1,0:T(8,128)(2,1)S(1)} all-to-all(bf16[8,32,256]{2,1,0:T(8,128)(2,1)S(1)} %pad_maximum_fusion.2), channel_id=1, replica_groups=mesh['sp'=64,'fs'=4,'tp'=2] {'fs','tp'}, dimensions={0} | all-to-all | bytes 262144 | tf_op jit(solution)/shard_map/all_to_all | solution.py:173
  221.2 3.7 %fusion.26 = bf16[32,2048]{1,0:T(8,128)(2,1)} fusion(f32[32,2048]{1,0:T(8,128)S(1)} %fusion.19, bf16[1024,4096]{1,0:T(8,128)(2,1)} %all-gather.5.cloned.1.call-done, bf16[8,4,8,128]{3,2,1,0:T(8,128)(2,1)S(1)} %get-tuple-element.337), kind=kOutput, calls=%fused_computation.29 | convolution fusion | flops 134348800 | bytes 4653056 | tf_op jit(solution)/shard_map/dot_general | solution.py:179
  (185 shorter events, 74.8 us)
Async XLA Ops:
  9.7 20.2 %all-to-all-start = ((bf16[8,32,2048]{2,1,0:T(8,128)(2,1)}), bf16[8,32,2048]{2,1,0:T(8,128)(2,1)S(1)}, u32[]{:S(2)}, u32[]{:S(2)}) async-start(bf16[8,32,2048]{2,1,0:T(8,128)(2,1)} %broadcast_in_dim.59), calls=%async_computation | async-start | bytes 2097152 | tf_op jit(solution)/shard_map/all_to_all | solution.py:19
  14.0 113.2 %all-gather.3.cloned.1.call-start = ((), (), s32[]{:S(2)}) async-start(), calls=%async_computation.2 | async-start | bytes 8519680 | tf_op jit(solution)/shard_map/all_gather | solution.py:35
  29.9 3.4 %copy-start = (bf16[128,2048]{1,0:T(8,128)(2,1)S(1)}, bf16[128,2048]{1,0:T(8,128)(2,1)}, u32[]{:S(2)}) copy-start(bf16[128,2048]{1,0:T(8,128)(2,1)} %param.28) | copy-start | bytes 1572868
  29.9 3.4 %copy-start.1 = (bf16[128,2048]{1,0:T(8,128)(2,1)S(1)}, bf16[128,2048]{1,0:T(8,128)(2,1)}, u32[]{:S(2)}) copy-start(bf16[128,2048]{1,0:T(8,128)(2,1)} %param.27) | copy-start | bytes 1572868
  32.3 2.3 %copy-start.4 = (s32[4]{0:T(128)S(1)}, s32[4]{0:T(128)}, u32[]{:S(2)}) copy-start(s32[4]{0:T(128)} %constant.143.clone) | copy-start | bytes 52
  32.3 16.6 %copy-start.2 = (f32[64]{0:T(128)S(1)}, f32[64]{0:T(128)}, u32[]{:S(2)}) copy-start(f32[64]{0:T(128)} %param.23) | copy-start | bytes 772
  33.3 184.9 %all-gather.5.cloned.1.call-start = ((), (), s32[]{:S(2)}) async-start(), calls=%async_computation.3 | async-start | bytes 9437184 | tf_op jit(solution)/shard_map/all_gather | solution.py:35
  46.3 5.5 %collective-permute-start = (bf16[15,128]{1,0:T(8,128)(2,1)S(1)}, bf16[15,128]{1,0:T(8,128)(2,1)S(1)}, u32[]{:S(2)}, u32[]{:S(2)}) collective-permute-start(bf16[15,128]{1,0:T(8,128)(2,1)S(1)} %slice.133), channel_id=1, source_target_pairs={{0,8},{8,16},{16,24},{24,32},{32,40},{40,48},{48,56},{56,64},{64,7... | collective-permute-start | bytes 11528 | tf_op jit(solution)/shard_map/ppermute | solution.py:45
  139.4 68.4 %copy-start.3 = (f32[128]{0:T(128)S(1)}, f32[128]{0:T(128)}, u32[]{:S(2)}) copy-start(f32[128]{0:T(128)} %param.26) | copy-start | bytes 1540
Sparse Core Ops, SparseCore 0:
  33.4 93.7 all-gather.2
  129.4 55.5 all-gather.4
where the time goes:
time: 233 us; the launch traced here: 232 us
  waiting for transfers between devices  93.1 us (40%)
  matrix products  60.6 us (26%)
  between operations  23.9 us (10%)
  local copies, waits for them, and re-layouts  14.7 us (6%)
  loops' own time  12.6 us (5%)
  blocking collectives  10.1 us (4%)
  other arithmetic  9.78 us (4%)
  starting transfers between devices  6.96 us (3%)
    all_gather x2, waiting for transfers between devices, side_by_side(): filled, at, done = (lax.all_gather(both, axis, axis=dim, tiled=True), 0, [])  75.1 us
    dot_general x16, matrix products, compute(): jnp.einsum('qhcd,khcd->hcqk', group_queries, key_block, preferred_element...  26 us
    dot_general x16, matrix products, compute(): jnp.einsum('hcqk,khe->hcqe', expo.astype(jnp.bfloat16), value_block, pref...  25.6 us
    all_to_all x1, waiting for transfers between devices, copy_for_each(): return lax.all_to_all(copies, axis, split_axis=0, concat_axis=0, tiled=True)  15.1 us
    another operation x1, loops' own time, body(): states = lax.fori_loop(0, key_count // block_rows, one_block, start_state)  11.6 us
    all_to_all x1, blocking collectives, body(): lax.all_to_all(mixed_local, ('fs', 'tp'), split_axis=0, concat_axis=1, ti...  10.1 us
    slice x1, local copies, waits for them, and re-layouts, side_by_side(): done.append(lax.slice_in_dim(filled, at, at + a.shape[along], axis=along))  6.44 us
    reshape x1, local copies, waits for them, and re-layouts, body(): value_heads = value_rows.reshape(key_count, heads_dev, value_dim)  5.72 us
  transfers between devices with their start and end apart: 4, of which 3 were waited for; matrix products, arithmetic and copies ran while one was open for 31% of the time, Pallas kernels for 0%

commit v1 on v0

v1 whole, which is shorter than its diff:
```python
import math

import jax
import jax.numpy as jnp
import numpy as np
from jax import lax
from jax.experimental import pallas as pl
from jax.experimental.pallas import tpu as pltpu
from jax.sharding import PartitionSpec as P

EPS = 1e-06
F32 = jnp.float32
BF16 = jnp.bfloat16
DH = 64
SIDE = 8
LANES = 128
EXTRA = 16
VMEM = 56 * 1024 * 1024
SCORE_SCALE = DH**-0.5 * math.log2(math.e)


def params(**kw):
    return pltpu.CompilerParams(vmem_limit_bytes=VMEM, **kw)


def rms_halves(raw, gain):
    left = lax.broadcasted_iota(jnp.int32, raw.shape, 1) < DH
    sq = raw * raw
    a = jnp.sum(jnp.where(left, sq, 0.0), axis=1, keepdims=True) * (1.0 / DH)
    b = jnp.sum(jnp.where(left, 0.0, sq), axis=1, keepdims=True) * (1.0 / DH)
    scale = jnp.where(left, lax.rsqrt(a + EPS), lax.rsqrt(b + EPS))
    return raw * scale * gain


def project_rows(x_ref, g_ref, wqk, wvp, qg_ref, kg_ref):
    chips, rows, width = x_ref.shape
    x = x_ref[...].reshape(chips * rows, width).astype(F32)
    mean = jnp.mean(x * x, axis=1, keepdims=True)
    normed = (x * lax.rsqrt(mean + EPS) * g_ref[...]).astype(BF16)
    qk = jnp.dot(normed, wqk, preferred_element_type=F32)
    vp = jnp.dot(normed, wvp, preferred_element_type=F32)
    twice = lambda ref: jnp.concatenate([ref[...], ref[...]], axis=1)
    q = rms_halves(qk[:, :LANES], twice(qg_ref) * SCORE_SCALE).astype(BF16)
    k = rms_halves(qk[:, LANES:], twice(kg_ref)).astype(BF16)
    return q, k, vp[:, :LANES].astype(BF16), vp[:, LANES:].astype(BF16)


def own_kernel(x_ref, g_ref, wq_ref, wk_ref, wv_ref, wp_ref, qg_ref, kg_ref, wqk_ref, wvp_ref, half_ref):
    wqk_ref[:, :LANES] = wq_ref[...]
    wqk_ref[:, LANES:] = wk_ref[...]
    wvp_ref[:, :LANES] = wv_ref[...]
    wvp_ref[:, LANES:] = wp_ref[...]
    parts = project_rows(x_ref, g_ref, wqk_ref[...], wvp_ref[...], qg_ref, kg_ref)
    for n, part in enumerate(parts):
        half_ref[n] = part


def far_kernel(core_ref, x_ref, half_ref, g_ref, wqk_ref, wvp_ref, qg_ref, kg_ref, q_ref, kv_ref, p_ref):
    chips, rows, _ = x_ref.shape
    copies = q_ref.shape[0]
    core = core_ref[0]
    far = project_rows(x_ref, g_ref, wqk_ref[...], wvp_ref[...], qg_ref, kg_ref)
    own = tuple(half_ref[n] for n in range(4))
    for (q, k, v, p), side in ((own, core), (far, 1 - core)):
        for i in range(chips):
            src = slice(i * rows, (i + 1) * rows)
            dst = pl.ds(pl.multiple_of((i * 2 + side) * rows, rows), rows)
            p_ref[dst, :] = p[src]
            for n in range(copies):
                q_ref[n, dst, :] = q[src]
                kv_ref[n, dst, :LANES] = k[src]
                kv_ref[n, dst, LANES:] = v[src]


def attend_kernel(at_ref, q_ref, kv_ref, o_ref, v1_ref, p_ref):
    blocks, rows, _ = kv_ref.shape
    for j in range(blocks):
        v1_ref[pl.ds(j * rows, rows), :LANES] = kv_ref[j, :, LANES:]
        v1_ref[pl.ds(j * rows, rows), LANES:] = jnp.ones((rows, LANES), BF16)
    k_first = at_ref[2]
    k_step = at_ref[3]

    def attend(i, q_block, count):
        q = q_ref[i]
        left = lax.broadcasted_iota(jnp.int32, q.shape, 1) < DH
        zero = jnp.zeros_like(q)
        q2 = jnp.concatenate([jnp.where(left, q, zero), jnp.where(left, zero, q)], axis=0)
        row = lax.broadcasted_iota(jnp.int32, (2 * rows, rows), 0) % rows
        ahead = lax.broadcasted_iota(jnp.int32, (2 * rows, rows), 1) - row
        for j in range(count):
            s = lax.dot_general(
                q2, kv_ref[j, :, :LANES], (((1,), (1,)), ((), ())), preferred_element_type=F32
            )
            room = (q_block - (k_first + k_step * j)) * rows
            p_ref[:, pl.ds(j * rows, rows)] = jnp.where(ahead <= room, jnp.exp2(s), 0.0).astype(BF16)
        out = jnp.dot(
            p_ref[:, : count * rows], v1_ref[: count * rows], preferred_element_type=F32
        )
        o_ref[i, :rows, :LANES] = out[:rows, :LANES].astype(BF16)
        o_ref[i, :rows, LANES:] = out[rows:, :LANES].astype(BF16)
        eye = lax.broadcasted_iota(jnp.int32, (LANES, LANES), 0) == lax.broadcasted_iota(
            jnp.int32, (LANES, LANES), 1
        )
        line = lax.broadcasted_iota(jnp.int32, (EXTRA, LANES), 0)
        for half in range(rows // LANES):
            tail = jnp.zeros((EXTRA, LANES), F32)
            for m in range(2):
                at = m * rows + half * LANES
                tot = out[at : at + LANES, LANES:]
                tot = jnp.sum(jnp.where(eye, tot, 0.0), axis=0, keepdims=True)
                high = tot.astype(BF16).astype(F32)
                tail = jnp.where(line == 2 * m, high, tail)
                tail = jnp.where(line == 2 * m + 1, tot - high, tail)
            o_ref[i, rows:, half * LANES : (half + 1) * LANES] = tail.astype(BF16)

    def one(i, carry):
        q_block = at_ref[0] + at_ref[1] * i
        many = k_first + k_step * (blocks // 2) <= q_block
        some = k_first <= q_block

        @pl.when(many)
        def _():
            attend(i, q_block, blocks)

        @pl.when(jnp.logical_and(some, jnp.logical_not(many)))
        def _():
            attend(i, q_block, blocks // 2)

        @pl.when(jnp.logical_not(some))
        def _():
            o_ref[i] = jnp.zeros(o_ref.shape[1:], BF16)

        return carry

    lax.fori_loop(0, o_ref.shape[0], one, 0)


def finish_kernel(at_ref, lam_ref, r_ref, pool_ref, halo_ref, hg_ref, wa_ref, wp_ref, keep_ref, send_ref, ext_ref, mix_ref):
    sources = r_ref.shape[0]
    chips, part, _ = keep_ref.shape
    rows = 2 * chips * part
    total = r_ref[0].astype(F32)
    for n in range(1, sources):
        total = total + r_ref[n].astype(F32)
    eye = lax.broadcasted_iota(jnp.int32, (LANES, LANES), 0) == lax.broadcasted_iota(
        jnp.int32, (LANES, LANES), 1
    )

    def column(m):
        cols = []
        for half in range(rows // LANES):
            at = slice(half * LANES, (half + 1) * LANES)
            line = total[rows + 2 * m : rows + 2 * m + 1, at] + total[rows + 2 * m + 1 : rows + 2 * m + 2, at]
            cols.append(jnp.sum(jnp.where(eye, line, 0.0), axis=1, keepdims=True))
        return jnp.concatenate(cols, axis=0)

    head = total[:rows, :LANES] / column(0) - lam_ref[0] * (total[:rows, LANES:] / column(1))
    mean = jnp.mean(head * head, axis=1, keepdims=True)
    attended = (head * lax.rsqrt(mean + EPS) * hg_ref[...]).astype(BF16)

    window = at_ref[1]
    halo = halo_ref.shape[0]
    ext_ref[:halo, :] = jnp.zeros((halo, LANES), F32)
    ext_ref[halo : 2 * halo, :] = halo_ref[...].astype(F32)
    ext_ref[2 * halo :, :] = pool_ref[...].astype(F32)
    pick = ext_ref[2 * halo :, :]
    own = pick
    span = 1
    total_rows = rows + 2 * halo
    while span < halo:
        wider = ext_ref[halo:, :] + ext_ref[halo - span : total_rows - span, :]
        ext_ref[halo:, :] = wider
        span *= 2
        pick = jnp.where(window == span, wider[halo:, :], pick)
    pos = at_ref[0] * rows + lax.broadcasted_iota(jnp.int32, (rows, LANES), 0)
    divisor = jnp.minimum(pos + 1, window).astype(F32)
    pooled = (pick / divisor - own).astype(BF16)

    mix_ref[:, :LANES] = attended
    mix_ref[:, LANES:] = pooled
    weights = jnp.concatenate([wa_ref[...], wp_ref[...]], axis=0)
    core = at_ref[2]
    for ref, side in ((send_ref, 1 - core), (keep_ref, core)):
        picked = [
            mix_ref[pl.ds(pl.multiple_of((n * 2 + side) * part, part), part), :] for n in range(chips)
        ]
        out = jnp.dot(jnp.concatenate(picked, axis=0), weights, preferred_element_type=F32)
        ref[...] = out.astype(BF16).reshape(ref.shape)


def plane_groups():
    index = np.arange(SIDE * SIDE * 2).reshape(SIDE, SIDE, 2)
    along_y = [[index[z, :, c].tolist() for z in range(SIDE)] for c in range(2)]
    along_z = [[index[:, y, c].tolist() for y in range(SIDE)] for c in range(2)]
    return along_y[0] + along_z[1], along_z[0] + along_y[1]


KEY_GROUPS, QUERY_GROUPS = plane_groups()


def in_vmem(x):
    return pltpu.with_memory_space_constraint(x, pltpu.VMEM)


def exchange(x, groups):
    return lax.all_to_all(
        x, ("sp", "tp"), split_axis=0, concat_axis=0, axis_index_groups=groups, tiled=True
    )


def body(
    tokens,
    norm_gain,
    w_query,
    w_key,
    w_value,
    w_pool,
    query_gain,
    key_gain,
    lambdas,
    head_gain,
    w_out_attn,
    w_out_pool,
):
    part, width = tokens.shape
    chips, cores = lax.axis_size("fs"), lax.axis_size("tp")
    rows = part * chips * cores
    place = lax.axis_index("sp")
    core = lax.axis_index("tp")
    z, y = place // SIDE, place % SIDE

    near = lax.all_gather(tokens, "fs", axis=0)
    far = lax.ppermute(near, "tp", [(0, 1), (1, 0)])

    vm = pl.BlockSpec(memory_space=pltpu.VMEM)
    sm = pl.BlockSpec(memory_space=pltpu.SMEM)
    here = core.astype(jnp.int32)[None]
    gains = (query_gain[None], key_gain[None])
    wqk, wvp, half = pl.pallas_call(
        own_kernel,
        in_specs=[vm] * 8,
        out_specs=[vm] * 3,
        out_shape=[
            pltpu.VMEM((width, 2 * LANES), BF16),
            pltpu.VMEM((width, 2 * LANES), BF16),
            pltpu.VMEM((4, chips * part, LANES), BF16),
        ],
        compiler_params=params(),
        name="own",
    )(in_vmem(near), norm_gain[None], w_query, w_key, w_value, w_pool, *gains)
    queries, keyvals, pool_input = pl.pallas_call(
        far_kernel,
        in_specs=[sm] + [vm] * 7,
        out_specs=[vm] * 3,
        out_shape=[
            pltpu.VMEM((SIDE, rows, LANES), BF16),
            pltpu.VMEM((SIDE, rows, 2 * LANES), BF16),
            pltpu.VMEM((rows, LANES), BF16),
        ],
        compiler_params=params(),
        name="far",
    )(here, in_vmem(far), in_vmem(half), norm_gain[None], in_vmem(wqk), in_vmem(wvp), *gains)

    devices = lax.axis_size("sp")
    halo = lax.ppermute(pool_input[rows - 16 :], "sp", [(i, i + 1) for i in range(devices - 1)])
    keyvals = exchange(keyvals, KEY_GROUPS)
    queries = exchange(queries, QUERY_GROUPS)

    across = core == 0
    where_at = jnp.stack(
        [
            jnp.where(across, y, SIDE * z),
            jnp.where(across, SIDE, 1),
            jnp.where(across, SIDE * z, y),
            jnp.where(across, 1, SIDE),
        ]
    ).astype(jnp.int32)
    partial = pl.pallas_call(
        attend_kernel,
        in_specs=[sm, vm, vm],
        out_specs=vm,
        out_shape=pltpu.VMEM((SIDE, rows + EXTRA, 2 * LANES), BF16),
        scratch_shapes=[
            pltpu.VMEM((SIDE * rows, 2 * LANES), BF16),
            pltpu.VMEM((2 * rows, SIDE * rows), BF16),
        ],
        compiler_params=params(),
        name="attend",
    )(where_at, in_vmem(queries), in_vmem(keyvals))

    partial = exchange(partial, QUERY_GROUPS)

    spot = jnp.stack([place, 2 << lax.axis_index("fs"), core]).astype(jnp.int32)
    keep, send = pl.pallas_call(
        finish_kernel,
        in_specs=[sm, sm] + [vm] * 6,
        out_specs=[vm, vm],
        out_shape=[pltpu.VMEM((chips, part, width), BF16)] * 2,
        scratch_shapes=[
            pltpu.VMEM((rows + 32, LANES), F32),
            pltpu.VMEM((rows, 2 * LANES), BF16),
        ],
        compiler_params=params(),
        name="finish",
    )(
        spot,
        lambdas,
        in_vmem(partial),
        in_vmem(pool_input),
        in_vmem(halo),
        head_gain[None],
        in_vmem(w_out_attn),
        in_vmem(w_out_pool),
    )

    other = lax.ppermute(send, "tp", [(0, 1), (1, 0)])
    mixed = (keep.astype(F32) + other.astype(F32)).astype(BF16)
    mixed = lax.all_to_all(mixed, "fs", split_axis=0, concat_axis=0, tiled=True)
    return jnp.sum(mixed.astype(F32), axis=0).astype(BF16)


def solution(mesh):
    return jax.shard_map(
        body,
        mesh=mesh,
        in_specs=(
            P(("sp", "fs", "tp"), None),
            P(),
            P(None, ("fs", "tp")),
            P(None, ("fs", "tp")),
            P(None, ("fs", "tp")),
            P(None, ("fs", "tp")),
            P(),
            P(),
            P(("fs", "tp")),
            P(),
            P(("fs", "tp"), None),
            P(("fs", "tp"), None),
        ),
        out_specs=P(("sp", "fs", "tp"), None),
        check_vma=False,
    )
```

time: 233 us -> 126 us (0.54)
  the two profiles are of different devices: /device:TPU:488 before, /device:TPU:1 now
where the time goes in v1:
time: 126 us; the launch traced here: 125 us
  blocking collectives  38.5 us (31%)
  starting transfers between devices  35.9 us (28%)
  waiting for transfers between devices  32.8 us (26%)
  Pallas kernels  14.9 us (12%)
  other arithmetic  2.21 us (2%)
    all_to_all x2, waiting for transfers between devices, exchange(): lax.all_to_all(x, ('sp', 'tp'), split_axis=0, concat_axis=0, axis_index_g...  24.6 us
    all_to_all x1, blocking collectives, exchange(): lax.all_to_all(x, ('sp', 'tp'), split_axis=0, concat_axis=0, axis_index_g...  14.8 us
    all_to_all x2, starting transfers between devices, exchange(): lax.all_to_all(x, ('sp', 'tp'), split_axis=0, concat_axis=0, axis_index_g...  12.7 us
    all_to_all x1, blocking collectives, body(): mixed = lax.all_to_all(mixed, 'fs', split_axis=0, concat_axis=0, tiled=True)  12.4 us
    all_gather x1, blocking collectives, body(): near = lax.all_gather(tokens, 'fs', axis=0)  11.3 us
    ppermute x1, starting transfers between devices, body(): far = lax.ppermute(near, 'tp', [(0, 1), (1, 0)])  10.5 us
    ppermute x1, starting transfers between devices, body(): other = lax.ppermute(send, 'tp', [(0, 1), (1, 0)])  9.52 us
    pallas_call x1, Pallas kernels, body(): pl.pallas_call(attend_kernel, in_specs=[sm, vm, vm], out_specs=vm, out_sh...  8.54 us
  transfers between devices with their start and end apart: 5, of which 4 were waited for; matrix products, arithmetic and copies ran while one was open for 1% of the time, Pallas kernels for 2%

profile of v1, /device:TPU:1, one launch (start us, length us, event | category | flops | bytes accessed | tf_op | source)
XLA Modules:
  0.0 125.0 jit_solution(12738778109258612577)
XLA Ops:
  0.0 11.3 %all-gather = bf16[128,2048]{1,0:T(8,128)(2,1)S(1)} all-gather(bf16[32,2048]{1,0:T(8,128)(2,1)} %param.12), channel_id=2, replica_groups=mesh['sp'=64,'fs'=4,'tp'=2] {'fs'}, dimensions={0}, use_global_device_ids=true | all-gather | bytes 655360 | tf_op jit(solution)/shard_map/all_gather | solution.py:232
  11.3 10.5 %collective-permute-start = (bf16[4,32,2048]{2,1,0:T(8,128)(2,1)S(1)}, bf16[4,32,2048]{2,1,0:T(8,128)(2,1)S(1)}, u32[]{:S(2)}, u32[]{:S(2)}) collective-permute-start(bf16[4,32,2048]{2,1,0:T(8,128)(2,1)S(1)} %bitcast.12), channel_id=1, source_target_pairs={{0,1},{1,0},{2,3},{3,2},{4,5},{5,4},{6,7},{7,6},{8,9},{9,8},{10,11... | collective-permute-start | bytes 1572872 | tf_op jit(solution)/shard_map/ppermute | solution.py:233
  21.7 2.4 %own.1 = (bf16[2048,256]{1,0:T(8,128)(2,1)S(1)}, bf16[2048,256]{1,0:T(8,128)(2,1)S(1)}, bf16[4,128,128]{2,1,0:T(8,128)(2,1)S(1)}) custom-call(bf16[4,32,2048]{2,1,0:T(8,128)(2,1)S(1)} %bitcast.13, f32[1,2048]{1,0:T(1,128)} %bitcast.14, bf16[2048,128]{1,0:T(8,128)(2,1)} %wq_ref.1, bf16[2048,128]{1,0:T(8,128)(2,1)} %wk_ref.1, bf16[2048,128]{1,0:T(8,128)(2,1)} %wv_ref.1, ...), custom_call_target="tpu_custom_call" | custom-call | tf_op jit(solution)/shard_map/own/pallas_call | solution.py:239
  24.2 0.0 collective-permute-done.x_ref
  24.2 2.4 %far.1 = (bf16[8,256,128]{2,1,0:T(8,128)(2,1)S(1)}, bf16[8,256,256]{2,1,0:T(8,128)(2,1)}, bf16[256,128]{1,0:T(8,128)(2,1)S(1)}) custom-call(s32[1]{0:T(128)} %bitcast.2.core_ref, bf16[4,32,2048]{2,1,0:T(8,128)(2,1)S(1)} %collective-permute-done.x_ref, bf16[4,128,128]{2,1,0:T(8,128)(2,1)S(1)} %get-tuple-element.13.half_ref, f32[1,2048]{1,0:T(1,128)} %bitcast.15, ...), custom_call_target="tpu_custom_call" | custom-call | tf_op jit(solution)/shard_map/far/pallas_call | solution.py:251
  26.6 14.8 %all_to_all.20.q_ref = bf16[8,256,128]{2,1,0:T(8,128)(2,1)S(1)} all-to-all(bf16[8,256,128]{2,1,0:T(8,128)(2,1)S(1)} %get-tuple-element.16), channel_id=1, replica_groups={{0,64,128,192,256,320,384,448},{8,72,136,200,264,328,392,456},{16,80,14..., dimensions={0} | all-to-all | bytes 1048576 | tf_op jit(solution)/shard_map/all_to_all | solution.py:206
  41.4 9.0 %all-to-all-start.1 = ((bf16[8,256,256]{2,1,0:T(8,128)(2,1)}), bf16[8,256,256]{2,1,0:T(8,128)(2,1)S(1)}, u32[]{:S(2)}, u32[]{:S(2)}) async-start(bf16[8,256,256]{2,1,0:T(8,128)(2,1)} %get-tuple-element.17), calls=%async_computation.1 | async-start | bytes 2097152 | tf_op jit(solution)/shard_map/all_to_all | solution.py:206
  50.4 0.7 pad_add_fusion.1.at_ref
  51.1 17.4 %all-to-all-done.1.kv_ref = bf16[8,256,256]{2,1,0:T(8,128)(2,1)S(1)} async-done(((bf16[8,256,256]{2,1,0:T(8,128)(2,1)}), bf16[8,256,256]{2,1,0:T(8,128)(2,1)S(1)}, u32[]{:S(2)}, u32[]{:S(2)}) %all-to-all-start.1) | async-done | bytes 1048608 | tf_op jit(solution)/shard_map/all_to_all | solution.py:206
  68.5 8.5 %attend.1 = bf16[8,272,256]{2,1,0:T(8,128)(2,1)} custom-call(s32[4]{0:T(128)} %pad_add_fusion.1.at_ref, bf16[8,256,128]{2,1,0:T(8,128)(2,1)S(1)} %all_to_all.20.q_ref, bf16[8,256,256]{2,1,0:T(8,128)(2,1)S(1)} %all-to-all-done.1.kv_ref), custom_call_target="tpu_custom_call" | custom-call | tf_op jit(solution)/shard_map/attend/pallas_call | solution.py:278
  77.0 0.0 copy-start
  77.0 3.7 %all-to-all-start.2 = ((bf16[8,272,256]{2,1,0:T(8,128)(2,1)}), bf16[8,272,256]{2,1,0:T(8,128)(2,1)S(1)}, u32[]{:S(2)}, u32[]{:S(2)}) async-start(bf16[8,272,256]{2,1,0:T(8,128)(2,1)} %attend.1), calls=%async_computation.2 | async-start | bytes 2228224 | tf_op jit(solution)/shard_map/all_to_all | solution.py:206
  80.8 3.2 %collective-permute-start.1 = (bf16[16,128]{1,0:T(8,128)(2,1)S(1)}, bf16[16,128]{1,0:T(8,128)(2,1)S(1)}, u32[]{:S(2)}, u32[]{:S(2)}) collective-permute-start(bf16[16,128]{1,0:T(8,128)(2,1)S(1)} %slice.3), channel_id=1, source_target_pairs={{0,8},{8,16},{16,24},{24,32},{32,40},{40,48},{48,56},{56,64},{64,7... | collective-permute-start | bytes 12296 | tf_op jit(solution)/shard_map/ppermute | solution.py:265
  84.0 0.7 pad_add_fusion.at_ref
  85.3 6.7 %collective-permute-done.1.halo_ref = bf16[16,128]{1,0:T(8,128)(2,1)S(1)} collective-permute-done((bf16[16,128]{1,0:T(8,128)(2,1)S(1)}, bf16[16,128]{1,0:T(8,128)(2,1)S(1)}, u32[]{:S(2)}, u32[]{:S(2)}) %collective-permute-start.1) | collective-permute-done | bytes 4128 | tf_op jit(solution)/shard_map/ppermute | solution.py:265
  92.1 7.2 %all-to-all-done.2.r_ref = bf16[8,272,256]{2,1,0:T(8,128)(2,1)S(1)} async-done(((bf16[8,272,256]{2,1,0:T(8,128)(2,1)}), bf16[8,272,256]{2,1,0:T(8,128)(2,1)S(1)}, u32[]{:S(2)}, u32[]{:S(2)}) %all-to-all-start.2) | async-done | bytes 1114144 | tf_op jit(solution)/shard_map/all_to_all | solution.py:206
  99.2 0.0 copy-done
  99.2 0.0 copy-done.1
  99.2 1.5 %finish.1 = (bf16[4,32,2048]{2,1,0:T(8,128)(2,1)S(1)}, bf16[4,32,2048]{2,1,0:T(8,128)(2,1)S(1)}) custom-call(s32[3]{0:T(128)} %pad_add_fusion.at_ref, f32[1]{0:T(128)S(6)} %copy.13.lam_ref, bf16[8,272,256]{2,1,0:T(8,128)(2,1)S(1)} %all-to-all-done.2.r_ref, bf16[256,128]{1,0:T(8,128)(2,1)S(1)} %get-tuple-element.18.pool_ref, ...), custom_call_target="tpu_custom_call" | custom-call | tf_op jit(solution)/shard_map/finish/pallas_call | solution.py:294
  100.7 9.5 %collective-permute-start.2 = (bf16[4,32,2048]{2,1,0:T(8,128)(2,1)S(1)}, bf16[4,32,2048]{2,1,0:T(8,128)(2,1)S(1)}, u32[]{:S(2)}, u32[]{:S(2)}) collective-permute-start(bf16[4,32,2048]{2,1,0:T(8,128)(2,1)S(1)} %get-tuple-element.20), channel_id=1, source_target_pairs={{0,1},{1,0},{2,3},{3,2},{4,5},{5,4},{6,7},{7,6},{8,9},{9,8},{10,11... | collective-permute-start | bytes 1572872 | tf_op jit(solution)/shard_map/ppermute | solution.py:316
  110.2 1.5 %collective-permute-done.2 = bf16[4,32,2048]{2,1,0:T(8,128)(2,1)S(1)} collective-permute-done((bf16[4,32,2048]{2,1,0:T(8,128)(2,1)S(1)}, bf16[4,32,2048]{2,1,0:T(8,128)(2,1)S(1)}, u32[]{:S(2)}, u32[]{:S(2)}) %collective-permute-start.2) | collective-permute-done | bytes 524320 | tf_op jit(solution)/shard_map/ppermute | solution.py:316
  111.8 0.1 add_convert_fusion
  111.9 12.4 %all_to_all.21 = bf16[4,32,2048]{2,1,0:T(8,128)(2,1)S(1)} all-to-all(bf16[4,32,2048]{2,1,0:T(8,128)(2,1)S(1)} %add_convert_fusion), channel_id=1, replica_groups=mesh['sp'=64,'fs'=4,'tp'=2] {'fs'}, dimensions={0} | all-to-all | bytes 1048576 | tf_op jit(solution)/shard_map/all_to_all | solution.py:318
  124.3 0.7 reduce_sum.12
  (2 shorter events, 0.0 us)
Async XLA Ops:
  11.3 12.9 %collective-permute-start = (bf16[4,32,2048]{2,1,0:T(8,128)(2,1)S(1)}, bf16[4,32,2048]{2,1,0:T(8,128)(2,1)S(1)}, u32[]{:S(2)}, u32[]{:S(2)}) collective-permute-start(bf16[4,32,2048]{2,1,0:T(8,128)(2,1)S(1)} %bitcast.12), channel_id=1, source_target_pairs={{0,1},{1,0},{2,3},{3,2},{4,5},{5,4},{6,7},{7,6},{8,9},{9,8},{10,11... | collective-permute-start | bytes 1572872 | tf_op jit(solution)/shard_map/ppermute | solution.py:233
  41.4 27.1 %all-to-all-start.1 = ((bf16[8,256,256]{2,1,0:T(8,128)(2,1)}), bf16[8,256,256]{2,1,0:T(8,128)(2,1)S(1)}, u32[]{:S(2)}, u32[]{:S(2)}) async-start(bf16[8,256,256]{2,1,0:T(8,128)(2,1)} %get-tuple-element.17), calls=%async_computation.1 | async-start | bytes 2097152 | tf_op jit(solution)/shard_map/all_to_all | solution.py:206
  77.0 22.2 %copy-start = (bf16[128,2048]{1,0:T(8,128)(2,1)S(1)}, bf16[128,2048]{1,0:T(8,128)(2,1)}, u32[]{:S(2)}) copy-start(bf16[128,2048]{1,0:T(8,128)(2,1)} %wa_ref.1) | copy-start | bytes 1572868
  77.0 22.2 %copy-start.1 = (bf16[128,2048]{1,0:T(8,128)(2,1)S(1)}, bf16[128,2048]{1,0:T(8,128)(2,1)}, u32[]{:S(2)}) copy-start(bf16[128,2048]{1,0:T(8,128)(2,1)} %wp_ref.3) | copy-start | bytes 1572868
  77.0 22.2 %all-to-all-start.2 = ((bf16[8,272,256]{2,1,0:T(8,128)(2,1)}), bf16[8,272,256]{2,1,0:T(8,128)(2,1)S(1)}, u32[]{:S(2)}, u32[]{:S(2)}) async-start(bf16[8,272,256]{2,1,0:T(8,128)(2,1)} %attend.1), calls=%async_computation.2 | async-start | bytes 2228224 | tf_op jit(solution)/shard_map/all_to_all | solution.py:206
  80.8 11.3 %collective-permute-start.1 = (bf16[16,128]{1,0:T(8,128)(2,1)S(1)}, bf16[16,128]{1,0:T(8,128)(2,1)S(1)}, u32[]{:S(2)}, u32[]{:S(2)}) collective-permute-start(bf16[16,128]{1,0:T(8,128)(2,1)S(1)} %slice.3), channel_id=1, source_target_pairs={{0,8},{8,16},{16,24},{24,32},{32,40},{40,48},{48,56},{56,64},{64,7... | collective-permute-start | bytes 12296 | tf_op jit(solution)/shard_map/ppermute | solution.py:265
  100.7 11.0 %collective-permute-start.2 = (bf16[4,32,2048]{2,1,0:T(8,128)(2,1)S(1)}, bf16[4,32,2048]{2,1,0:T(8,128)(2,1)S(1)}, u32[]{:S(2)}, u32[]{:S(2)}) collective-permute-start(bf16[4,32,2048]{2,1,0:T(8,128)(2,1)S(1)} %get-tuple-element.20), channel_id=1, source_target_pairs={{0,1},{1,0},{2,3},{3,2},{4,5},{5,4},{6,7},{7,6},{8,9},{9,8},{10,11... | collective-permute-start | bytes 1572872 | tf_op jit(solution)/shard_map/ppermute | solution.py:316

commit v2 on v1

--- a/solution.py
+++ b/solution.py
@@ -7,6 +7,7 @@
 from jax.experimental import pallas as pl
 from jax.experimental.pallas import tpu as pltpu
 from jax.sharding import PartitionSpec as P
+
 
 EPS = 1e-06
 F32 = jnp.float32
@@ -57,7 +58,7 @@
 
 def far_kernel(core_ref, x_ref, half_ref, g_ref, wqk_ref, wvp_ref, qg_ref, kg_ref, q_ref, kv_ref, p_ref):
     chips, rows, _ = x_ref.shape
-    copies = q_ref.shape[0]
+    copies = kv_ref.shape[0]
     core = core_ref[0]
     far = project_rows(x_ref, g_ref, wqk_ref[...], wvp_ref[...], qg_ref, kg_ref)
     own = tuple(half_ref[n] for n in range(4))
@@ -66,8 +67,8 @@
             src = slice(i * rows, (i + 1) * rows)
             dst = pl.ds(pl.multiple_of((i * 2 + side) * rows, rows), rows)
             p_ref[dst, :] = p[src]
+            q_ref[dst, :] = q[src]
             for n in range(copies):
-                q_ref[n, dst, :] = q[src]
                 kv_ref[n, dst, :LANES] = k[src]
                 kv_ref[n, dst, LANES:] = v[src]
 
@@ -80,8 +81,8 @@
     k_first = at_ref[2]
     k_step = at_ref[3]
 
-    def attend(i, q_block, count):
-        q = q_ref[i]
+    def attend(step, i, q_block, count):
+        q = q_ref[step]
         left = lax.broadcasted_iota(jnp.int32, q.shape, 1) < DH
         zero = jnp.zeros_like(q)
         q2 = jnp.concatenate([jnp.where(left, q, zero), jnp.where(left, zero, q)], axis=0)
@@ -113,18 +114,20 @@
                 tail = jnp.where(line == 2 * m + 1, tot - high, tail)
             o_ref[i, rows:, half * LANES : (half + 1) * LANES] = tail.astype(BF16)
 
-    def one(i, carry):
+    def one(step, carry):
+        odd = step % 2
+        i = step - odd + jnp.where(at_ref[4] == 1, 1 - odd, odd)
         q_block = at_ref[0] + at_ref[1] * i
         many = k_first + k_step * (blocks // 2) <= q_block
         some = k_first <= q_block
 
         @pl.when(many)
         def _():
-            attend(i, q_block, blocks)
+            attend(step, i, q_block, blocks)
 
         @pl.when(jnp.logical_and(some, jnp.logical_not(many)))
         def _():
-            attend(i, q_block, blocks // 2)
+            attend(step, i, q_block, blocks // 2)
 
         @pl.when(jnp.logical_not(some))
         def _():
@@ -196,6 +199,8 @@
 
 
 KEY_GROUPS, QUERY_GROUPS = plane_groups()
+QUERY_PAIRS = [(g[i], g[i ^ 1]) for g in QUERY_GROUPS for i in range(SIDE)]
+QUERY_FOURS = [g[parity::2] for g in QUERY_GROUPS for parity in range(2)]
 
 
 def in_vmem(x):
@@ -253,7 +258,7 @@
         in_specs=[sm] + [vm] * 7,
         out_specs=[vm] * 3,
         out_shape=[
-            pltpu.VMEM((SIDE, rows, LANES), BF16),
+            pltpu.VMEM((rows, LANES), BF16),
             pltpu.VMEM((SIDE, rows, 2 * LANES), BF16),
             pltpu.VMEM((rows, LANES), BF16),
         ],
@@ -264,7 +269,9 @@
     devices = lax.axis_size("sp")
     halo = lax.ppermute(pool_input[rows - 16 :], "sp", [(i, i + 1) for i in range(devices - 1)])
     keyvals = exchange(keyvals, KEY_GROUPS)
-    queries = exchange(queries, QUERY_GROUPS)
+    beside = lax.ppermute(queries, ("sp", "tp"), QUERY_PAIRS)
+    queries = jnp.stack([queries, beside])
+    queries = lax.all_gather(queries, ("sp", "tp"), axis=0, axis_index_groups=QUERY_FOURS, tiled=True)
 
     across = core == 0
     where_at = jnp.stack(
@@ -273,6 +280,7 @@
             jnp.where(across, SIDE, 1),
             jnp.where(across, SIDE * z, y),
             jnp.where(across, 1, SIDE),
+            jnp.where(across, z, y) % 2,
         ]
     ).astype(jnp.int32)
     partial = pl.pallas_call(

time: 126 us -> 113 us (0.90)
  the two profiles are of different devices: /device:TPU:1 before, /device:TPU:32 now
where the time goes in v2:
time: 113 us; the launch traced here: 112 us
  blocking collectives  47.6 us (42%)
  starting transfers between devices  21.5 us (19%)
  waiting for transfers between devices  21 us (19%)
  Pallas kernels  19.3 us (17%)
  other arithmetic  1.5 us (1%)
    all_gather x1, blocking collectives, body(): lax.all_gather(queries, ('sp', 'tp'), axis=0, axis_index_groups=QUERY_FOU...  20.4 us
    all_to_all x1, blocking collectives, body(): mixed = lax.all_to_all(mixed, 'fs', split_axis=0, concat_axis=0, tiled=True)  13.8 us
    all_gather x1, blocking collectives, body(): near = lax.all_gather(tokens, 'fs', axis=0)  13.3 us
    pallas_call x1, Pallas kernels, body(): pl.pallas_call(attend_kernel, in_specs=[sm, vm, vm], out_specs=vm, out_sh...  13 us
    all_to_all x2, waiting for transfers between devices, exchange(): lax.all_to_all(x, ('sp', 'tp'), split_axis=0, concat_axis=0, axis_index_g...  12.8 us
    all_to_all x2, starting transfers between devices, exchange(): lax.all_to_all(x, ('sp', 'tp'), split_axis=0, concat_axis=0, axis_index_g...  12.3 us
    ppermute x1, waiting for transfers between devices, body(): beside = lax.ppermute(queries, ('sp', 'tp'), QUERY_PAIRS)  3.26 us
    ppermute x1, waiting for transfers between devices, body(): lax.ppermute(pool_input[rows - 16:], 'sp', [(i, i + 1) for i in range(dev...  2.97 us
  transfers between devices with their start and end apart: 6, of which 4 were waited for; matrix products, arithmetic and copies ran while one was open for 1% of the time, Pallas kernels for 2%

profile of v2, /device:TPU:32, one launch (start us, length us, event | category | flops | bytes accessed | tf_op | source)
XLA Modules:
  0.0 112.3 jit_solution(6105778323666243660)
XLA Ops:
  0.0 13.3 %all-gather = bf16[128,2048]{1,0:T(8,128)(2,1)S(1)} all-gather(bf16[32,2048]{1,0:T(8,128)(2,1)} %param.12), channel_id=2, replica_groups=mesh['sp'=64,'fs'=4,'tp'=2] {'fs'}, dimensions={0}, use_global_device_ids=true | all-gather | bytes 655360 | tf_op jit(solution)/shard_map/all_gather | solution.py:237
  13.3 1.9 %collective-permute-start = (bf16[4,32,2048]{2,1,0:T(8,128)(2,1)S(1)}, bf16[4,32,2048]{2,1,0:T(8,128)(2,1)S(1)}, u32[]{:S(2)}, u32[]{:S(2)}) collective-permute-start(bf16[4,32,2048]{2,1,0:T(8,128)(2,1)S(1)} %bitcast.15), channel_id=1, source_target_pairs={{0,1},{1,0},{2,3},{3,2},{4,5},{5,4},{6,7},{7,6},{8,9},{9,8},{10,11... | collective-permute-start | bytes 1572872 | tf_op jit(solution)/shard_map/ppermute | solution.py:238
  15.3 2.4 %own.1 = (bf16[2048,256]{1,0:T(8,128)(2,1)S(1)}, bf16[2048,256]{1,0:T(8,128)(2,1)S(1)}, bf16[4,128,128]{2,1,0:T(8,128)(2,1)S(1)}) custom-call(bf16[4,32,2048]{2,1,0:T(8,128)(2,1)S(1)} %bitcast.16, f32[1,2048]{1,0:T(1,128)} %bitcast.19, bf16[2048,128]{1,0:T(8,128)(2,1)} %wq_ref.1, bf16[2048,128]{1,0:T(8,128)(2,1)} %wk_ref.1, bf16[2048,128]{1,0:T(8,128)(2,1)} %wv_ref.1, ...), custom_call_target="tpu_custom_call" | custom-call | tf_op jit(solution)/shard_map/own/pallas_call | solution.py:244
  17.7 0.0 collective-permute-done.x_ref
  17.7 2.4 %far.1 = (bf16[256,128]{1,0:T(8,128)(2,1)S(1)}, bf16[8,256,256]{2,1,0:T(8,128)(2,1)}, bf16[256,128]{1,0:T(8,128)(2,1)S(1)}) custom-call(s32[1]{0:T(128)} %bitcast.2.core_ref, bf16[4,32,2048]{2,1,0:T(8,128)(2,1)S(1)} %collective-permute-done.x_ref, bf16[4,128,128]{2,1,0:T(8,128)(2,1)S(1)} %get-tuple-element.13.half_ref, f32[1,2048]{1,0:T(1,128)} %bitcast.20, ...), custom_call_target="tpu_custom_call" | custom-call | tf_op jit(solution)/shard_map/far/pallas_call | solution.py:256
  20.1 8.6 %all-to-all-start = ((bf16[8,256,256]{2,1,0:T(8,128)(2,1)}), bf16[8,256,256]{2,1,0:T(8,128)(2,1)S(1)}, u32[]{:S(2)}, u32[]{:S(2)}) async-start(bf16[8,256,256]{2,1,0:T(8,128)(2,1)} %get-tuple-element.17), calls=%async_computation | async-start | bytes 2097152 | tf_op jit(solution)/shard_map/all_to_all | solution.py:211
  28.7 2.9 %collective-permute-start.1 = (bf16[256,128]{1,0:T(8,128)(2,1)S(1)}, bf16[256,128]{1,0:T(8,128)(2,1)S(1)}, u32[]{:S(2)}, u32[]{:S(2)}) collective-permute-start(bf16[256,128]{1,0:T(8,128)(2,1)S(1)} %get-tuple-element.16), channel_id=1, source_target_pairs={{0,64},{64,0},{128,192},{192,128},{256,320},{320,256},{384,448},{4... | collective-permute-start | bytes 196616 | tf_op jit(solution)/shard_map/ppermute | solution.py:272
  31.7 0.6 stack.48.at_ref
  32.3 3.3 %collective-permute-done.1 = bf16[256,128]{1,0:T(8,128)(2,1)S(1)} collective-permute-done((bf16[256,128]{1,0:T(8,128)(2,1)S(1)}, bf16[256,128]{1,0:T(8,128)(2,1)S(1)}, u32[]{:S(2)}, u32[]{:S(2)}) %collective-permute-start.1) | collective-permute-done | bytes 65568 | tf_op jit(solution)/shard_map/ppermute | solution.py:272
  35.6 20.4 %all_gather.11.q_ref = bf16[8,256,128]{2,1,0:T(8,128)(2,1)S(1)} all-gather(bf16[2,256,128]{2,1,0:T(8,128)(2,1)S(1)} %pad_maximum_fusion), channel_id=1, replica_groups={{0,128,256,384},{64,192,320,448},{8,136,264,392},{72,200,328,456},{16,1..., dimensions={0}, use_global_device_ids=true | all-gather | bytes 655360 | tf_op jit(solution)/shard_map/all_gather | solution.py:274
  56.0 0.0 all-to-all-done.kv_ref
  56.0 13.0 %attend.1 = bf16[8,272,256]{2,1,0:T(8,128)(2,1)} custom-call(s32[5]{0:T(128)} %stack.48.at_ref, bf16[8,256,128]{2,1,0:T(8,128)(2,1)S(1)} %all_gather.11.q_ref, bf16[8,256,256]{2,1,0:T(8,128)(2,1)S(1)} %all-to-all-done.kv_ref), custom_call_target="tpu_custom_call" | custom-call | tf_op jit(solution)/shard_map/attend/pallas_call | solution.py:286
  69.0 3.7 %all-to-all-start.1 = ((bf16[8,272,256]{2,1,0:T(8,128)(2,1)}), bf16[8,272,256]{2,1,0:T(8,128)(2,1)S(1)}, u32[]{:S(2)}, u32[]{:S(2)}) async-start(bf16[8,272,256]{2,1,0:T(8,128)(2,1)} %attend.1), calls=%async_computation.1 | async-start | bytes 2228224 | tf_op jit(solution)/shard_map/all_to_all | solution.py:211
  72.7 2.5 %collective-permute-start.2 = (bf16[16,128]{1,0:T(8,128)(2,1)S(1)}, bf16[16,128]{1,0:T(8,128)(2,1)S(1)}, u32[]{:S(2)}, u32[]{:S(2)}) collective-permute-start(bf16[16,128]{1,0:T(8,128)(2,1)S(1)} %slice.3), channel_id=1, source_target_pairs={{0,8},{8,16},{16,24},{24,32},{32,40},{40,48},{48,56},{56,64},{64,7... | collective-permute-start | bytes 12296 | tf_op jit(solution)/shard_map/ppermute | solution.py:270
  75.2 0.6 pad_add_fusion.at_ref
  76.4 3.0 %collective-permute-done.2.halo_ref = bf16[16,128]{1,0:T(8,128)(2,1)S(1)} collective-permute-done((bf16[16,128]{1,0:T(8,128)(2,1)S(1)}, bf16[16,128]{1,0:T(8,128)(2,1)S(1)}, u32[]{:S(2)}, u32[]{:S(2)}) %collective-permute-start.2) | collective-permute-done | bytes 4128 | tf_op jit(solution)/shard_map/ppermute | solution.py:270
  79.4 12.8 %all-to-all-done.1.r_ref = bf16[8,272,256]{2,1,0:T(8,128)(2,1)S(1)} async-done(((bf16[8,272,256]{2,1,0:T(8,128)(2,1)}), bf16[8,272,256]{2,1,0:T(8,128)(2,1)S(1)}, u32[]{:S(2)}, u32[]{:S(2)}) %all-to-all-start.1) | async-done | bytes 1114144 | tf_op jit(solution)/shard_map/all_to_all | solution.py:211
  92.3 0.0 copy-done
  92.3 1.5 %finish.1 = (bf16[4,32,2048]{2,1,0:T(8,128)(2,1)S(1)}, bf16[4,32,2048]{2,1,0:T(8,128)(2,1)S(1)}) custom-call(s32[3]{0:T(128)} %pad_add_fusion.at_ref, f32[1]{0:T(128)S(6)} %copy.13.lam_ref, bf16[8,272,256]{2,1,0:T(8,128)(2,1)S(1)} %all-to-all-done.1.r_ref, bf16[256,128]{1,0:T(8,128)(2,1)S(1)} %get-tuple-element.18.pool_ref, ...), custom_call_target="tpu_custom_call" | custom-call | tf_op jit(solution)/shard_map/finish/pallas_call | solution.py:302
  93.8 1.9 %collective-permute-start.3 = (bf16[4,32,2048]{2,1,0:T(8,128)(2,1)S(1)}, bf16[4,32,2048]{2,1,0:T(8,128)(2,1)S(1)}, u32[]{:S(2)}, u32[]{:S(2)}) collective-permute-start(bf16[4,32,2048]{2,1,0:T(8,128)(2,1)S(1)} %get-tuple-element.20), channel_id=1, source_target_pairs={{0,1},{1,0},{2,3},{3,2},{4,5},{5,4},{6,7},{7,6},{8,9},{9,8},{10,11... | collective-permute-start | bytes 1572872 | tf_op jit(solution)/shard_map/ppermute | solution.py:324
  95.7 1.9 %collective-permute-done.3 = bf16[4,32,2048]{2,1,0:T(8,128)(2,1)S(1)} collective-permute-done((bf16[4,32,2048]{2,1,0:T(8,128)(2,1)S(1)}, bf16[4,32,2048]{2,1,0:T(8,128)(2,1)S(1)}, u32[]{:S(2)}, u32[]{:S(2)}) %collective-permute-start.3) | collective-permute-done | bytes 524320 | tf_op jit(solution)/shard_map/ppermute | solution.py:324
  97.6 0.1 add_convert_fusion
  97.7 13.8 %all_to_all.15 = bf16[4,32,2048]{2,1,0:T(8,128)(2,1)S(1)} all-to-all(bf16[4,32,2048]{2,1,0:T(8,128)(2,1)S(1)} %add_convert_fusion), channel_id=1, replica_groups=mesh['sp'=64,'fs'=4,'tp'=2] {'fs'}, dimensions={0} | all-to-all | bytes 1048576 | tf_op jit(solution)/shard_map/all_to_all | solution.py:326
  111.5 0.7 reduce_sum.12
  (5 shorter events, 0.0 us)
Async XLA Ops:
  13.3 4.4 %collective-permute-start = (bf16[4,32,2048]{2,1,0:T(8,128)(2,1)S(1)}, bf16[4,32,2048]{2,1,0:T(8,128)(2,1)S(1)}, u32[]{:S(2)}, u32[]{:S(2)}) collective-permute-start(bf16[4,32,2048]{2,1,0:T(8,128)(2,1)S(1)} %bitcast.15), channel_id=1, source_target_pairs={{0,1},{1,0},{2,3},{3,2},{4,5},{5,4},{6,7},{7,6},{8,9},{9,8},{10,11... | collective-permute-start | bytes 1572872 | tf_op jit(solution)/shard_map/ppermute | solution.py:238
  20.1 35.9 %all-to-all-start = ((bf16[8,256,256]{2,1,0:T(8,128)(2,1)}), bf16[8,256,256]{2,1,0:T(8,128)(2,1)S(1)}, u32[]{:S(2)}, u32[]{:S(2)}) async-start(bf16[8,256,256]{2,1,0:T(8,128)(2,1)} %get-tuple-element.17), calls=%async_computation | async-start | bytes 2097152 | tf_op jit(solution)/shard_map/all_to_all | solution.py:211
  28.7 6.8 %collective-permute-start.1 = (bf16[256,128]{1,0:T(8,128)(2,1)S(1)}, bf16[256,128]{1,0:T(8,128)(2,1)S(1)}, u32[]{:S(2)}, u32[]{:S(2)}) collective-permute-start(bf16[256,128]{1,0:T(8,128)(2,1)S(1)} %get-tuple-element.16), channel_id=1, source_target_pairs={{0,64},{64,0},{128,192},{192,128},{256,320},{320,256},{384,448},{4... | collective-permute-start | bytes 196616 | tf_op jit(solution)/shard_map/ppermute | solution.py:272
  69.0 23.3 %copy-start = (bf16[128,2048]{1,0:T(8,128)(2,1)S(1)}, bf16[128,2048]{1,0:T(8,128)(2,1)}, u32[]{:S(2)}) copy-start(bf16[128,2048]{1,0:T(8,128)(2,1)} %wa_ref.1) | copy-start | bytes 1572868
  69.0 23.3 %copy-start.1 = (bf16[128,2048]{1,0:T(8,128)(2,1)S(1)}, bf16[128,2048]{1,0:T(8,128)(2,1)}, u32[]{:S(2)}) copy-start(bf16[128,2048]{1,0:T(8,128)(2,1)} %wp_ref.3) | copy-start | bytes 1572868
  69.0 23.3 %all-to-all-start.1 = ((bf16[8,272,256]{2,1,0:T(8,128)(2,1)}), bf16[8,272,256]{2,1,0:T(8,128)(2,1)S(1)}, u32[]{:S(2)}, u32[]{:S(2)}) async-start(bf16[8,272,256]{2,1,0:T(8,128)(2,1)} %attend.1), calls=%async_computation.1 | async-start | bytes 2228224 | tf_op jit(solution)/shard_map/all_to_all | solution.py:211
  72.7 6.7 %collective-permute-start.2 = (bf16[16,128]{1,0:T(8,128)(2,1)S(1)}, bf16[16,128]{1,0:T(8,128)(2,1)S(1)}, u32[]{:S(2)}, u32[]{:S(2)}) collective-permute-start(bf16[16,128]{1,0:T(8,128)(2,1)S(1)} %slice.3), channel_id=1, source_target_pairs={{0,8},{8,16},{16,24},{24,32},{32,40},{40,48},{48,56},{56,64},{64,7... | collective-permute-start | bytes 12296 | tf_op jit(solution)/shard_map/ppermute | solution.py:270
  93.8 3.8 %collective-permute-start.3 = (bf16[4,32,2048]{2,1,0:T(8,128)(2,1)S(1)}, bf16[4,32,2048]{2,1,0:T(8,128)(2,1)S(1)}, u32[]{:S(2)}, u32[]{:S(2)}) collective-permute-start(bf16[4,32,2048]{2,1,0:T(8,128)(2,1)S(1)} %get-tuple-element.20), channel_id=1, source_target_pairs={{0,1},{1,0},{2,3},{3,2},{4,5},{5,4},{6,7},{7,6},{8,9},{9,8},{10,11... | collective-permute-start | bytes 1572872 | tf_op jit(solution)/shard_map/ppermute | solution.py:324

commit v3 on v2

--- a/solution.py
+++ b/solution.py
@@ -73,30 +73,59 @@
                 kv_ref[n, dst, LANES:] = v[src]
 
 
-def attend_kernel(at_ref, q_ref, kv_ref, o_ref, v1_ref, p_ref):
+def early_kernel(at_ref, q_ref, kv_ref, o_ref, v1_ref, *held):
     blocks, rows, _ = kv_ref.shape
     for j in range(blocks):
         v1_ref[pl.ds(j * rows, rows), :LANES] = kv_ref[j, :, LANES:]
         v1_ref[pl.ds(j * rows, rows), LANES:] = jnp.ones((rows, LANES), BF16)
+    attend_half(1, at_ref, q_ref, kv_ref, o_ref, v1_ref, held)
+
+
+def late_kernel(at_ref, q_ref, kv_ref, v1_ref, o_ref, *held):
+    attend_half(0, at_ref, q_ref, kv_ref, o_ref, v1_ref, held)
+
+
+def merge_kernel(a_ref, b_ref, o_ref):
+    blocks, rows, _ = o_ref.shape
+    rows -= EXTRA
+    line = lax.broadcasted_iota(jnp.int32, (EXTRA, 2 * LANES), 0)
+    for n in range(blocks):
+        o_ref[n, :rows] = (a_ref[n, :rows].astype(F32) + b_ref[n, :rows].astype(F32)).astype(BF16)
+        both = a_ref[n, rows:].astype(F32) + b_ref[n, rows:].astype(F32)
+        tail = jnp.zeros((EXTRA, 2 * LANES), F32)
+        for m in range(2):
+            tot = both[2 * m : 2 * m + 1] + both[2 * m + 1 : 2 * m + 2]
+            high = tot.astype(BF16).astype(F32)
+            tail = jnp.where(line == 2 * m, high, tail)
+            tail = jnp.where(line == 2 * m + 1, tot - high, tail)
+        o_ref[n, rows:] = tail.astype(BF16)
+
+
+def attend_half(other, at_ref, q_ref, kv_ref, o_ref, v1_ref, held):
+    blocks, rows, _ = kv_ref.shape
+    tall = 2 * rows
     k_first = at_ref[2]
     k_step = at_ref[3]
 
-    def attend(step, i, q_block, count):
-        q = q_ref[step]
+    def score(i, p_ref):
+        q_block = at_ref[0] + at_ref[1] * (2 * i + jnp.where(at_ref[4] == 1, 1 - other, other))
+        q = q_ref[2 * i + other]
         left = lax.broadcasted_iota(jnp.int32, q.shape, 1) < DH
         zero = jnp.zeros_like(q)
         q2 = jnp.concatenate([jnp.where(left, q, zero), jnp.where(left, zero, q)], axis=0)
-        row = lax.broadcasted_iota(jnp.int32, (2 * rows, rows), 0) % rows
-        ahead = lax.broadcasted_iota(jnp.int32, (2 * rows, rows), 1) - row
-        for j in range(count):
+        row = lax.broadcasted_iota(jnp.int32, (tall, rows), 0) % rows
+        ahead = lax.broadcasted_iota(jnp.int32, (tall, rows), 1) - row
+        for j in range(blocks):
             s = lax.dot_general(
                 q2, kv_ref[j, :, :LANES], (((1,), (1,)), ((), ())), preferred_element_type=F32
             )
             room = (q_block - (k_first + k_step * j)) * rows
-            p_ref[:, pl.ds(j * rows, rows)] = jnp.where(ahead <= room, jnp.exp2(s), 0.0).astype(BF16)
-        out = jnp.dot(
-            p_ref[:, : count * rows], v1_ref[: count * rows], preferred_element_type=F32
-        )
+            p_ref[:, pl.ds(j * rows, rows)] = jnp.where(
+                ahead <= room, jnp.exp2(s), 0.0
+            ).astype(BF16)
+
+    def gather(i, p_ref):
+        out = jnp.dot(p_ref[...], v1_ref[...], preferred_element_type=F32)
         o_ref[i, :rows, :LANES] = out[:rows, :LANES].astype(BF16)
         o_ref[i, :rows, LANES:] = out[rows:, :LANES].astype(BF16)
         eye = lax.broadcasted_iota(jnp.int32, (LANES, LANES), 0) == lax.broadcasted_iota(
@@ -114,34 +143,30 @@
                 tail = jnp.where(line == 2 * m + 1, tot - high, tail)
             o_ref[i, rows:, half * LANES : (half + 1) * LANES] = tail.astype(BF16)
 
-    def one(step, carry):
-        odd = step % 2
-        i = step - odd + jnp.where(at_ref[4] == 1, 1 - odd, odd)
-        q_block = at_ref[0] + at_ref[1] * i
-        many = k_first + k_step * (blocks // 2) <= q_block
-        some = k_first <= q_block
-
-        @pl.when(many)
-        def _():
-            attend(step, i, q_block, blocks)
-
-        @pl.when(jnp.logical_and(some, jnp.logical_not(many)))
-        def _():
-            attend(step, i, q_block, blocks // 2)
-
-        @pl.when(jnp.logical_not(some))
-        def _():
-            o_ref[i] = jnp.zeros(o_ref.shape[1:], BF16)
-
-        return carry
-
-    lax.fori_loop(0, o_ref.shape[0], one, 0)
-
-
-def finish_kernel(at_ref, lam_ref, r_ref, pool_ref, halo_ref, hg_ref, wa_ref, wp_ref, keep_ref, send_ref, ext_ref, mix_ref):
+    count = o_ref.shape[0]
+
+    def span(begin):
+        score(begin, held[0])
+        for i in range(begin, count):
+            if i + 1 < count:
+                score(i + 1, held[(i - begin + 1) % 2])
+            gather(i, held[(i - begin) % 2])
+
+    unseen = k_first > at_ref[0] + at_ref[1] * (count - 1)
+
+    @pl.when(unseen)
+    def _():
+        o_ref[: count // 2] = jnp.zeros((count // 2, *o_ref.shape[1:]), BF16)
+        span(count // 2)
+
+    @pl.when(jnp.logical_not(unseen))
+    def _():
+        span(0)
+
+
+def finish_kernel(at_ref, lam_ref, r_ref, pool_ref, halo_ref, hg_ref, mix_ref, ext_ref):
     sources = r_ref.shape[0]
-    chips, part, _ = keep_ref.shape
-    rows = 2 * chips * part
+    rows = mix_ref.shape[0]
     total = r_ref[0].astype(F32)
     for n in range(1, sources):
         total = total + r_ref[n].astype(F32)
@@ -161,7 +186,7 @@
     mean = jnp.mean(head * head, axis=1, keepdims=True)
     attended = (head * lax.rsqrt(mean + EPS) * hg_ref[...]).astype(BF16)
 
-    window = at_ref[1]
+    window = at_ref[6]
     halo = halo_ref.shape[0]
     ext_ref[:halo, :] = jnp.zeros((halo, LANES), F32)
     ext_ref[halo : 2 * halo, :] = halo_ref[...].astype(F32)
@@ -175,20 +200,31 @@
         ext_ref[halo:, :] = wider
         span *= 2
         pick = jnp.where(window == span, wider[halo:, :], pick)
-    pos = at_ref[0] * rows + lax.broadcasted_iota(jnp.int32, (rows, LANES), 0)
+    pos = at_ref[5] * rows + lax.broadcasted_iota(jnp.int32, (rows, LANES), 0)
     divisor = jnp.minimum(pos + 1, window).astype(F32)
     pooled = (pick / divisor - own).astype(BF16)
 
     mix_ref[:, :LANES] = attended
     mix_ref[:, LANES:] = pooled
-    weights = jnp.concatenate([wa_ref[...], wp_ref[...]], axis=0)
-    core = at_ref[2]
-    for ref, side in ((send_ref, 1 - core), (keep_ref, core)):
-        picked = [
-            mix_ref[pl.ds(pl.multiple_of((n * 2 + side) * part, part), part), :] for n in range(chips)
-        ]
-        out = jnp.dot(jnp.concatenate(picked, axis=0), weights, preferred_element_type=F32)
-        ref[...] = out.astype(BF16).reshape(ref.shape)
+
+
+def output_kernel(at_ref, mix_ref, wa_ref, wp_ref, far_wa_ref, far_wp_ref, o_ref):
+    chips, part, _ = o_ref.shape
+    core = at_ref[7]
+
+    def product(side, attn, pool):
+        rows = jnp.concatenate(
+            [
+                mix_ref[side, pl.ds(pl.multiple_of((n * 2 + core) * part, part), part), :]
+                for n in range(chips)
+            ],
+            axis=0,
+        )
+        weights = jnp.concatenate([attn[...], pool[...]], axis=0)
+        return jnp.dot(rows, weights, preferred_element_type=F32)
+
+    out = product(core, wa_ref, wp_ref) + product(1 - core, far_wa_ref, far_wp_ref)
+    o_ref[...] = out.astype(BF16).reshape(o_ref.shape)
 
 
 def plane_groups():
@@ -281,48 +317,70 @@
             jnp.where(across, SIDE * z, y),
             jnp.where(across, 1, SIDE),
             jnp.where(across, z, y) % 2,
+            place,
+            2 << lax.axis_index("fs"),
+            core,
         ]
     ).astype(jnp.int32)
+    half_shape = pltpu.VMEM((SIDE // 2, rows + EXTRA, 2 * LANES), BF16)
+    weights_scratch = pltpu.VMEM((2 * rows, SIDE * rows), BF16)
+    queries, keyvals = in_vmem(queries), in_vmem(keyvals)
+    early, values_ones = pl.pallas_call(
+        early_kernel,
+        in_specs=[sm, vm, vm],
+        out_specs=[vm, vm],
+        out_shape=[half_shape, pltpu.VMEM((SIDE * rows, 2 * LANES), BF16)],
+        scratch_shapes=[weights_scratch] * 2,
+        compiler_params=params(),
+        name="early",
+    )(where_at, queries, keyvals)
+    passed = lax.ppermute(early, ("sp", "tp"), QUERY_PAIRS)
+    late = pl.pallas_call(
+        late_kernel,
+        in_specs=[sm, vm, vm, vm],
+        out_specs=vm,
+        out_shape=half_shape,
+        scratch_shapes=[weights_scratch] * 2,
+        compiler_params=params(),
+        name="late",
+    )(where_at, queries, keyvals, in_vmem(values_ones))
     partial = pl.pallas_call(
-        attend_kernel,
-        in_specs=[sm, vm, vm],
+        merge_kernel,
+        in_specs=[vm, vm],
         out_specs=vm,
-        out_shape=pltpu.VMEM((SIDE, rows + EXTRA, 2 * LANES), BF16),
-        scratch_shapes=[
-            pltpu.VMEM((SIDE * rows, 2 * LANES), BF16),
-            pltpu.VMEM((2 * rows, SIDE * rows), BF16),
-        ],
-        compiler_params=params(),
-        name="attend",
-    )(where_at, in_vmem(queries), in_vmem(keyvals))
-
-    partial = exchange(partial, QUERY_GROUPS)
-
-    spot = jnp.stack([place, 2 << lax.axis_index("fs"), core]).astype(jnp.int32)
-    keep, send = pl.pallas_call(
+        out_shape=half_shape,
+        compiler_params=params(),
+        name="merge",
+    )(in_vmem(late), in_vmem(passed))
+    partial = exchange(partial, QUERY_FOURS)
+    far_attn = lax.ppermute(w_out_attn, "tp", [(0, 1), (1, 0)])
+    far_pool = lax.ppermute(w_out_pool, "tp", [(0, 1), (1, 0)])
+
+    mixed = pl.pallas_call(
         finish_kernel,
-        in_specs=[sm, sm] + [vm] * 6,
-        out_specs=[vm, vm],
-        out_shape=[pltpu.VMEM((chips, part, width), BF16)] * 2,
-        scratch_shapes=[
-            pltpu.VMEM((rows + 32, LANES), F32),
-            pltpu.VMEM((rows, 2 * LANES), BF16),
-        ],
+        in_specs=[sm, sm] + [vm] * 4,
+        out_specs=vm,
+        out_shape=pltpu.VMEM((rows, 2 * LANES), BF16),
+        scratch_shapes=[pltpu.VMEM((rows + 32, LANES), F32)],
         compiler_params=params(),
         name="finish",
     )(
-        spot,
+        where_at,
         lambdas,
         in_vmem(partial),
         in_vmem(pool_input),
         in_vmem(halo),
         head_gain[None],
-        in_vmem(w_out_attn),
-        in_vmem(w_out_pool),
     )
-
-    other = lax.ppermute(send, "tp", [(0, 1), (1, 0)])
-    mixed = (keep.astype(F32) + other.astype(F32)).astype(BF16)
+    mixed = lax.all_gather(mixed, "tp", axis=0)
+    mixed = pl.pallas_call(
+        output_kernel,
+        in_specs=[sm] + [vm] * 5,
+        out_specs=vm,
+        out_shape=pltpu.VMEM((chips, part, width), BF16),
+        compiler_params=params(),
+        name="output",
+    )(where_at, in_vmem(mixed), *map(in_vmem, (w_out_attn, w_out_pool, far_attn, far_pool)))
     mixed = lax.all_to_all(mixed, "fs", split_axis=0, concat_axis=0, tiled=True)
     return jnp.sum(mixed.astype(F32), axis=0).astype(BF16)
 

time: 113 us -> 110 us (0.973)
  the two profiles are of different devices: /device:TPU:32 before, /device:TPU:24 now
where the time goes in v3:
time: 110 us; the launch traced here: 109 us
  blocking collectives  49.5 us (45%)
  starting transfers between devices  30.4 us (28%)
  Pallas kernels  19.1 us (17%)
  waiting for transfers between devices  8.18 us (7%)
    all_gather x1, blocking collectives, body(): lax.all_gather(queries, ('sp', 'tp'), axis=0, axis_index_groups=QUERY_FOU...  20.1 us
    all_to_all x1, blocking collectives, body(): mixed = lax.all_to_all(mixed, 'fs', split_axis=0, concat_axis=0, tiled=True)  14 us
    all_gather x1, blocking collectives, body(): near = lax.all_gather(tokens, 'fs', axis=0)  13.3 us
    all_to_all x2, starting transfers between devices, exchange(): lax.all_to_all(x, ('sp', 'tp'), split_axis=0, concat_axis=0, axis_index_g...  12.3 us
    pallas_call x1, Pallas kernels, body(): pl.pallas_call(late_kernel, in_specs=[sm, vm, vm, vm], out_specs=vm, out_...  5.53 us
    pallas_call x1, Pallas kernels, body(): pl.pallas_call(early_kernel, in_specs=[sm, vm, vm], out_specs=[vm, vm], o...  5.49 us
    ppermute x1, starting transfers between devices, body(): passed = lax.ppermute(early, ('sp', 'tp'), QUERY_PAIRS)  4.47 us
    ppermute x1, starting transfers between devices, body(): lax.ppermute(pool_input[rows - 16:], 'sp', [(i, i + 1) for i in range(dev...  4.47 us
  transfers between devices with their start and end apart: 8, of which 4 were waited for; matrix products, arithmetic and copies ran while one was open for 1% of the time, Pallas kernels for 8%

profile of v3, /device:TPU:24, one launch (start us, length us, event | category | flops | bytes accessed | tf_op | source)
XLA Modules:
  0.0 109.3 jit_solution(12460134344524760040)
XLA Ops:
  0.0 13.3 %all-gather = bf16[128,2048]{1,0:T(8,128)(2,1)S(1)} all-gather(bf16[32,2048]{1,0:T(8,128)(2,1)} %param.12), channel_id=2, replica_groups=mesh['sp'=64,'fs'=4,'tp'=2] {'fs'}, dimensions={0}, use_global_device_ids=true | all-gather | bytes 655360 | tf_op jit(solution)/shard_map/all_gather | solution.py:273
  13.3 1.9 %collective-permute-start = (bf16[4,32,2048]{2,1,0:T(8,128)(2,1)S(1)}, bf16[4,32,2048]{2,1,0:T(8,128)(2,1)S(1)}, u32[]{:S(2)}, u32[]{:S(2)}) collective-permute-start(bf16[4,32,2048]{2,1,0:T(8,128)(2,1)S(1)} %bitcast.16), channel_id=1, source_target_pairs={{0,1},{1,0},{2,3},{3,2},{4,5},{5,4},{6,7},{7,6},{8,9},{9,8},{10,11... | collective-permute-start | bytes 1572872 | tf_op jit(solution)/shard_map/ppermute | solution.py:274
  15.3 2.4 %own.1 = (bf16[2048,256]{1,0:T(8,128)(2,1)S(1)}, bf16[2048,256]{1,0:T(8,128)(2,1)S(1)}, bf16[4,128,128]{2,1,0:T(8,128)(2,1)S(1)}) custom-call(bf16[4,32,2048]{2,1,0:T(8,128)(2,1)S(1)} %bitcast.17, f32[1,2048]{1,0:T(1,128)} %bitcast.21, bf16[2048,128]{1,0:T(8,128)(2,1)} %wq_ref.1, bf16[2048,128]{1,0:T(8,128)(2,1)} %wk_ref.1, bf16[2048,128]{1,0:T(8,128)(2,1)} %wv_ref.1, ...), custom_call_target="tpu_custom_call" | custom-call | tf_op jit(solution)/shard_map/own/pallas_call | solution.py:280
  17.7 2.4 %far.1 = (bf16[256,128]{1,0:T(8,128)(2,1)S(1)}, bf16[8,256,256]{2,1,0:T(8,128)(2,1)}, bf16[256,128]{1,0:T(8,128)(2,1)S(1)}) custom-call(s32[1]{0:T(128)} %bitcast.7.core_ref, bf16[4,32,2048]{2,1,0:T(8,128)(2,1)S(1)} %collective-permute-done.x_ref, bf16[4,128,128]{2,1,0:T(8,128)(2,1)S(1)} %get-tuple-element.13.half_ref, f32[1,2048]{1,0:T(1,128)} %bitcast.22, ...), custom_call_target="tpu_custom_call" | custom-call | tf_op jit(solution)/shard_map/far/pallas_call | solution.py:292
  20.1 8.7 %all-to-all-start = ((bf16[8,256,256]{2,1,0:T(8,128)(2,1)}), bf16[8,256,256]{2,1,0:T(8,128)(2,1)S(1)}, u32[]{:S(2)}, u32[]{:S(2)}) async-start(bf16[8,256,256]{2,1,0:T(8,128)(2,1)} %get-tuple-element.17), calls=%async_computation | async-start | bytes 2097152 | tf_op jit(solution)/shard_map/all_to_all | solution.py:247
  28.8 2.9 %collective-permute-start.1 = (bf16[256,128]{1,0:T(8,128)(2,1)S(1)}, bf16[256,128]{1,0:T(8,128)(2,1)S(1)}, u32[]{:S(2)}, u32[]{:S(2)}) collective-permute-start(bf16[256,128]{1,0:T(8,128)(2,1)S(1)} %get-tuple-element.16), channel_id=1, source_target_pairs={{0,64},{64,0},{128,192},{192,128},{256,320},{320,256},{384,448},{4... | collective-permute-start | bytes 196616 | tf_op jit(solution)/shard_map/ppermute | solution.py:308
  31.8 0.7 stack.44.at_ref
  32.5 3.6 %collective-permute-done.1 = bf16[256,128]{1,0:T(8,128)(2,1)S(1)} collective-permute-done((bf16[256,128]{1,0:T(8,128)(2,1)S(1)}, bf16[256,128]{1,0:T(8,128)(2,1)S(1)}, u32[]{:S(2)}, u32[]{:S(2)}) %collective-permute-start.1) | collective-permute-done | bytes 65568 | tf_op jit(solution)/shard_map/ppermute | solution.py:308
  36.1 20.1 %all_gather.17.q_ref = bf16[8,256,128]{2,1,0:T(8,128)(2,1)S(1)} all-gather(bf16[2,256,128]{2,1,0:T(8,128)(2,1)S(1)} %pad_maximum_fusion), channel_id=1, replica_groups={{0,128,256,384},{64,192,320,448},{8,136,264,392},{72,200,328,456},{16,1..., dimensions={0}, use_global_device_ids=true | all-gather | bytes 655360 | tf_op jit(solution)/shard_map/all_gather | solution.py:310
  56.2 5.5 %early.1 = (bf16[4,272,256]{2,1,0:T(8,128)(2,1)S(1)}, bf16[2048,256]{1,0:T(8,128)(2,1)S(1)}) custom-call(s32[8]{0:T(128)} %stack.44.at_ref, bf16[8,256,128]{2,1,0:T(8,128)(2,1)S(1)} %all_gather.17.q_ref, bf16[8,256,256]{2,1,0:T(8,128)(2,1)S(1)} %all-to-all-done.kv_ref), custom_call_target="tpu_custom_call" | custom-call | tf_op jit(solution)/shard_map/early/pallas_call | solution.py:328
  61.7 4.5 %collective-permute-start.2 = (bf16[4,272,256]{2,1,0:T(8,128)(2,1)S(1)}, bf16[4,272,256]{2,1,0:T(8,128)(2,1)S(1)}, u32[]{:S(2)}, u32[]{:S(2)}) collective-permute-start(bf16[4,272,256]{2,1,0:T(8,128)(2,1)S(1)} %get-tuple-element.19), channel_id=1, source_target_pairs={{0,64},{64,0},{128,192},{192,128},{256,320},{320,256},{384,448},{4... | collective-permute-start | bytes 1671176 | tf_op jit(solution)/shard_map/ppermute | solution.py:337
  66.2 5.5 %late.1.a_ref = bf16[4,272,256]{2,1,0:T(8,128)(2,1)S(1)} custom-call(s32[8]{0:T(128)} %stack.44.at_ref, bf16[8,256,128]{2,1,0:T(8,128)(2,1)S(1)} %all_gather.17.q_ref, bf16[8,256,256]{2,1,0:T(8,128)(2,1)S(1)} %all-to-all-done.kv_ref, bf16[2048,256]{1,0:T(8,128)(2,1)S(1)} %get-tuple-element.18.v1_ref), custom_call_target="tpu_custom_call" | custom-call | tf_op jit(solution)/shard_map/late/pallas_call | solution.py:338
  71.7 2.0 %collective-permute-done.2.b_ref = bf16[4,272,256]{2,1,0:T(8,128)(2,1)S(1)} collective-permute-done((bf16[4,272,256]{2,1,0:T(8,128)(2,1)S(1)}, bf16[4,272,256]{2,1,0:T(8,128)(2,1)S(1)}, u32[]{:S(2)}, u32[]{:S(2)}) %collective-permute-start.2) | collective-permute-done | bytes 557088 | tf_op jit(solution)/shard_map/ppermute | solution.py:337
  73.7 0.9 merge.1
  74.6 3.6 %all-to-all-start.1 = ((bf16[4,272,256]{2,1,0:T(8,128)(2,1)}), bf16[4,272,256]{2,1,0:T(8,128)(2,1)S(1)}, u32[]{:S(2)}, u32[]{:S(2)}) async-start(bf16[4,272,256]{2,1,0:T(8,128)(2,1)} %merge.1), calls=%async_computation.1 | async-start | bytes 1114112 | tf_op jit(solution)/shard_map/all_to_all | solution.py:247
  78.3 1.9 %collective-permute-start.4 = (bf16[128,2048]{1,0:T(8,128)(2,1)S(1)}, bf16[128,2048]{1,0:T(8,128)(2,1)S(1)}, u32[]{:S(2)}, u32[]{:S(2)}) collective-permute-start(bf16[128,2048]{1,0:T(8,128)(2,1)S(1)} %copy-done), channel_id=1, source_target_pairs={{0,1},{1,0},{2,3},{3,2},{4,5},{5,4},{6,7},{7,6},{8,9},{9,8},{10,11... | collective-permute-start | bytes 1572872 | tf_op jit(solution)/shard_map/ppermute | solution.py:356
  80.2 2.4 %collective-permute-start.5 = (bf16[128,2048]{1,0:T(8,128)(2,1)S(1)}, bf16[128,2048]{1,0:T(8,128)(2,1)S(1)}, u32[]{:S(2)}, u32[]{:S(2)}) collective-permute-start(bf16[128,2048]{1,0:T(8,128)(2,1)S(1)} %copy-done.1), channel_id=1, source_target_pairs={{0,1},{1,0},{2,3},{3,2},{4,5},{5,4},{6,7},{7,6},{8,9},{9,8},{10,11... | collective-permute-start | bytes 1572872 | tf_op jit(solution)/shard_map/ppermute | solution.py:357
  82.6 4.5 %collective-permute-start.3 = (bf16[16,128]{1,0:T(8,128)(2,1)S(1)}, bf16[16,128]{1,0:T(8,128)(2,1)S(1)}, u32[]{:S(2)}, u32[]{:S(2)}) collective-permute-start(bf16[16,128]{1,0:T(8,128)(2,1)S(1)} %slice.3), channel_id=1, source_target_pairs={{0,8},{8,16},{16,24},{24,32},{32,40},{40,48},{48,56},{56,64},{64,7... | collective-permute-start | bytes 12296 | tf_op jit(solution)/shard_map/ppermute | solution.py:306
  88.4 2.0 %all-to-all-done.1.r_ref = bf16[4,272,256]{2,1,0:T(8,128)(2,1)S(1)} async-done(((bf16[4,272,256]{2,1,0:T(8,128)(2,1)}), bf16[4,272,256]{2,1,0:T(8,128)(2,1)S(1)}, u32[]{:S(2)}, u32[]{:S(2)}) %all-to-all-start.1) | async-done | bytes 557088 | tf_op jit(solution)/shard_map/all_to_all | solution.py:247
  90.4 1.1 %finish.1 = bf16[256,256]{1,0:T(8,128)(2,1)S(1)} custom-call(s32[8]{0:T(128)} %stack.44.at_ref, f32[1]{0:T(128)S(6)} %copy.13.lam_ref, bf16[4,272,256]{2,1,0:T(8,128)(2,1)S(1)} %all-to-all-done.1.r_ref, bf16[256,128]{1,0:T(8,128)(2,1)S(1)} %get-tuple-element.20.pool_ref, bf16[16,128]{1,0:T(8,128)(2,1)S(1)} %collective-permute-done.3.halo_ref, f32[1,128]{1,0:T(1,128)} %bitcast.27), custom_call_target="tpu_custom_call" | custom-call | tf_op jit(solution)/shard_map/finish/pallas_call | solution.py:359
  91.5 2.0 %all-gather.1 = bf16[512,256]{1,0:T(8,128)(2,1)S(1)} all-gather(bf16[256,256]{1,0:T(8,128)(2,1)S(1)} %finish.1), channel_id=3, replica_groups=mesh['sp'=64,'fs'=4,'tp'=2] {'tp'}, dimensions={0}, use_global_device_ids=true | all-gather | bytes 393216 | tf_op jit(solution)/shard_map/all_gather | solution.py:375
  93.5 1.1 %output.1 = bf16[4,32,2048]{2,1,0:T(8,128)(2,1)S(1)} custom-call(s32[8]{0:T(128)} %stack.44.at_ref, bf16[2,256,256]{2,1,0:T(8,128)(2,1)S(1)} %bitcast.18, bf16[128,2048]{1,0:T(8,128)(2,1)S(1)} %copy-done, bf16[128,2048]{1,0:T(8,128)(2,1)S(1)} %copy-done.1, bf16[128,2048]{1,0:T(8,128)(2,1)S(1)} %collective-permute-done.4.far_wa_ref, ...), custom_call_target="tpu_custom_call" | custom-call | tf_op jit(solution)/shard_map/output/pallas_call | solution.py:376
  94.6 14.0 %all_to_all.15 = bf16[4,32,2048]{2,1,0:T(8,128)(2,1)S(1)} all-to-all(bf16[4,32,2048]{2,1,0:T(8,128)(2,1)S(1)} %output.1), channel_id=1, replica_groups=mesh['sp'=64,'fs'=4,'tp'=2] {'fs'}, dimensions={0} | all-to-all | bytes 1048576 | tf_op jit(solution)/shard_map/all_to_all | solution.py:384
  108.6 0.7 reduce_sum.12
  (11 shorter events, 0.7 us)
Async XLA Ops:
  13.3 4.4 %collective-permute-start = (bf16[4,32,2048]{2,1,0:T(8,128)(2,1)S(1)}, bf16[4,32,2048]{2,1,0:T(8,128)(2,1)S(1)}, u32[]{:S(2)}, u32[]{:S(2)}) collective-permute-start(bf16[4,32,2048]{2,1,0:T(8,128)(2,1)S(1)} %bitcast.16), channel_id=1, source_target_pairs={{0,1},{1,0},{2,3},{3,2},{4,5},{5,4},{6,7},{7,6},{8,9},{9,8},{10,11... | collective-permute-start | bytes 1572872 | tf_op jit(solution)/shard_map/ppermute | solution.py:274
  20.1 36.1 %all-to-all-start = ((bf16[8,256,256]{2,1,0:T(8,128)(2,1)}), bf16[8,256,256]{2,1,0:T(8,128)(2,1)S(1)}, u32[]{:S(2)}, u32[]{:S(2)}) async-start(bf16[8,256,256]{2,1,0:T(8,128)(2,1)} %get-tuple-element.17), calls=%async_computation | async-start | bytes 2097152 | tf_op jit(solution)/shard_map/all_to_all | solution.py:247
  28.8 7.2 %collective-permute-start.1 = (bf16[256,128]{1,0:T(8,128)(2,1)S(1)}, bf16[256,128]{1,0:T(8,128)(2,1)S(1)}, u32[]{:S(2)}, u32[]{:S(2)}) collective-permute-start(bf16[256,128]{1,0:T(8,128)(2,1)S(1)} %get-tuple-element.16), channel_id=1, source_target_pairs={{0,64},{64,0},{128,192},{192,128},{256,320},{320,256},{384,448},{4... | collective-permute-start | bytes 196616 | tf_op jit(solution)/shard_map/ppermute | solution.py:308
  61.7 12.0 %collective-permute-start.2 = (bf16[4,272,256]{2,1,0:T(8,128)(2,1)S(1)}, bf16[4,272,256]{2,1,0:T(8,128)(2,1)S(1)}, u32[]{:S(2)}, u32[]{:S(2)}) collective-permute-start(bf16[4,272,256]{2,1,0:T(8,128)(2,1)S(1)} %get-tuple-element.19), channel_id=1, source_target_pairs={{0,64},{64,0},{128,192},{192,128},{256,320},{320,256},{384,448},{4... | collective-permute-start | bytes 1671176 | tf_op jit(solution)/shard_map/ppermute | solution.py:337
  74.6 3.6 %copy-start = (bf16[128,2048]{1,0:T(8,128)(2,1)S(1)}, bf16[128,2048]{1,0:T(8,128)(2,1)}, u32[]{:S(2)}) copy-start(bf16[128,2048]{1,0:T(8,128)(2,1)} %wa_ref.1) | copy-start | bytes 1572868
  74.6 5.6 %copy-start.1 = (bf16[128,2048]{1,0:T(8,128)(2,1)S(1)}, bf16[128,2048]{1,0:T(8,128)(2,1)}, u32[]{:S(2)}) copy-start(bf16[128,2048]{1,0:T(8,128)(2,1)} %wp_ref.3) | copy-start | bytes 1572868
  74.6 15.7 %all-to-all-start.1 = ((bf16[4,272,256]{2,1,0:T(8,128)(2,1)}), bf16[4,272,256]{2,1,0:T(8,128)(2,1)S(1)}, u32[]{:S(2)}, u32[]{:S(2)}) async-start(bf16[4,272,256]{2,1,0:T(8,128)(2,1)} %merge.1), calls=%async_computation.1 | async-start | bytes 1114112 | tf_op jit(solution)/shard_map/all_to_all | solution.py:247
  78.3 15.2 %collective-permute-start.4 = (bf16[128,2048]{1,0:T(8,128)(2,1)S(1)}, bf16[128,2048]{1,0:T(8,128)(2,1)S(1)}, u32[]{:S(2)}, u32[]{:S(2)}) collective-permute-start(bf16[128,2048]{1,0:T(8,128)(2,1)S(1)} %copy-done), channel_id=1, source_target_pairs={{0,1},{1,0},{2,3},{3,2},{4,5},{5,4},{6,7},{7,6},{8,9},{9,8},{10,11... | collective-permute-start | bytes 1572872 | tf_op jit(solution)/shard_map/ppermute | solution.py:356
  80.2 13.3 %collective-permute-start.5 = (bf16[128,2048]{1,0:T(8,128)(2,1)S(1)}, bf16[128,2048]{1,0:T(8,128)(2,1)S(1)}, u32[]{:S(2)}, u32[]{:S(2)}) collective-permute-start(bf16[128,2048]{1,0:T(8,128)(2,1)S(1)} %copy-done.1), channel_id=1, source_target_pairs={{0,1},{1,0},{2,3},{3,2},{4,5},{5,4},{6,7},{7,6},{8,9},{9,8},{10,11... | collective-permute-start | bytes 1572872 | tf_op jit(solution)/shard_map/ppermute | solution.py:357
  82.6 5.8 %collective-permute-start.3 = (bf16[16,128]{1,0:T(8,128)(2,1)S(1)}, bf16[16,128]{1,0:T(8,128)(2,1)S(1)}, u32[]{:S(2)}, u32[]{:S(2)}) collective-permute-start(bf16[16,128]{1,0:T(8,128)(2,1)S(1)} %slice.3), channel_id=1, source_target_pairs={{0,8},{8,16},{16,24},{24,32},{32,40},{40,48},{48,56},{56,64},{64,7... | collective-permute-start | bytes 12296 | tf_op jit(solution)/shard_map/ppermute | solution.py:306
